TPU v7x, 512 devices: a whole 4x4x16 slice. The times are simulated.
512 devices in a mesh: sp: 128 (over z, x, core), tp: 4 (over y).
Axes of the slice: x: 4, y: 4, z: 16, core: 2. Of those that a mesh axis runs over, the one named last changes fastest.
Arguments:
- tokens: bfloat16 [65536, 2048], P('sp', 'tp'), may hold values from -72 to 72
- w_query: bfloat16 [2048, 1024], P('sp', 'tp'), may hold values from -0.125 to 0.125
- w_key: bfloat16 [2048, 256], P('sp', 'tp'), may hold values from -0.125 to 0.125
- w_value: bfloat16 [2048, 256], P('sp', 'tp'), may hold values from -0.125 to 0.125
- w_pool_in: bfloat16 [2048, 1024], P('sp', 'tp'), may hold values from -0.125 to 0.125
- sink: float32 [16], P('tp'), may hold values from 3 to 7
- w_pool: bfloat16 [4, 256, 256], P('tp'), may hold values from -0.375 to 0.375
- pool_scale: float32 [1024], P('tp'), may hold values from 0.1 to 1.9
- w_out_attn: bfloat16 [1024, 2048], P('tp', 'sp'), may hold values from -0.5 to 0.5
- w_out_pool: bfloat16 [1024, 2048], P('tp', 'sp'), may hold values from -0.125 to 0.125
- out_gain: float32 [2048], P('tp'), may hold values from 0.1 to 1.9
Outputs:
- mixed: bfloat16 [65536, 2048], P('sp', 'tp')
All inputs are finite; a program needn't handle non-finite values.
Results may differ from a plain program's by a relative error of at most 0.012.
The roundings to bfloat16 on the way count: a program that leaves them out, or rounds other values in their place, can miss the bound.
Values may be sent and summed in bfloat16 or wider, within the bound.
A program may use at most 64 MiB of HBM per device.

v0:
```python
import jax
import jax.numpy as jnp
from jax import lax
from jax.sharding import Mesh
from jax.sharding import PartitionSpec as P

HEAD_DIM = 64
POOL_GROUPS = 4
WINDOW = 128
SP = ("sp_0", "sp_1", "sp_2")


epsilon = 1e-05
masked_score = -1e30


def from_everyone(shard, axis):
    count = lax.axis_size(axis)
    return lax.all_to_all(
        jnp.broadcast_to(shard[None], (count, *shard.shape)), axis, 0, 0, tiled=True
    )


def in_order(pieces, dim):
    dims = list(pieces.shape[1:])
    dims[dim] *= pieces.shape[0]
    return jnp.moveaxis(pieces, 0, dim).reshape(dims)


def gather_axes(shard, axes, dim):
    far, near = axes
    first = from_everyone(shard, far)
    pieces = jnp.swapaxes(from_everyone(first, near), 0, 1)
    return in_order(pieces.reshape(-1, *shard.shape), dim)


def gather_directly(shard, axis, dim):
    pieces = from_everyone(shard, axis)
    return in_order(pieces, dim)


def side_by_side(arrays, axis, dim, along):
    both = jnp.concatenate(arrays, axis=along)
    out, at, gathered = (lax.all_gather(both, axis, axis=dim, tiled=True), 0, [])
    for a in arrays:
        gathered.append(lax.slice_in_dim(out, at, at + a.shape[along], axis=along))
        at += a.shape[along]
    return tuple(gathered)


def padded(cells, sides, width):
    for axis, dim in sides:
        count = lax.axis_size(axis)
        ends = count - 1
        head = lax.slice_in_dim(cells, 0, width, axis=dim)
        tail = lax.slice_in_dim(cells, cells.shape[dim] - width, cells.shape[dim], axis=dim)
        cells = jnp.concatenate(
            [
                lax.ppermute(tail, axis, [(i, (i + 1) % count) for i in range(ends)]),
                cells,
                lax.ppermute(head, axis, [((i + 1) % count, i) for i in range(ends)]),
            ],
            axis=dim,
        )
    return cells


def cut_along(shard, dim, count):
    dims = shard.shape
    pieces = shard.reshape(*dims[:dim], count, dims[dim] // count, *dims[dim + 1 :])
    return jnp.moveaxis(pieces, dim, 0)


def sent_and_summed(shard, axis, dim):
    count = lax.axis_size(axis)
    pieces = lax.all_to_all(cut_along(shard, dim, count), axis, 0, 0, tiled=True)
    return jnp.sum(pieces.astype(jnp.float32), axis=0)


def of_everyone(shard, axis):
    everything = from_everyone(shard, axis)
    return jnp.sum(everything, axis=0)


def in_one(arrays, axis):
    ends = [0]
    for a in arrays:
        ends.append(ends[-1] + a.size)
    so_far = of_everyone(jnp.concatenate([a.ravel() for a in arrays]), axis)
    return tuple((so_far[b:e].reshape(a.shape) for a, b, e in zip(arrays, ends, ends[1:])))


def make_projector(gathered, pieces):
    piece_query, piece_key, piece_value, piece_chan = pieces
    joined = jnp.concatenate([piece_key, piece_value], axis=1)
    return (
        jnp.dot(gathered, piece_query, preferred_element_type=jnp.float32),
        jnp.dot(gathered, joined, preferred_element_type=jnp.float32),
        jnp.dot(gathered, piece_chan, preferred_element_type=jnp.float32),
    )


def attend_local(query, keys_ext, sinks, offset, seq_len, key_cols):
    tok_rows, query_cols = query.shape
    kv_local = key_cols // HEAD_DIM
    group = query_cols // key_cols
    block_count = tok_rows // WINDOW
    stacked = keys_ext.reshape(block_count + 2, WINDOW, 2 * key_cols)
    banded = jnp.concatenate([stacked[:-2], stacked[1:-1], stacked[2:]], axis=1)
    key_band = banded[:, :, :key_cols].reshape(block_count, 3 * WINDOW, kv_local, HEAD_DIM)
    value_band = banded[:, :, key_cols:].reshape(block_count, 3 * WINDOW, kv_local, HEAD_DIM)
    query_blocks = query.reshape(block_count, WINDOW, kv_local, group, HEAD_DIM)
    scores = jnp.einsum(
        "nqkgd,nskd->nkgqs", query_blocks, key_band, preferred_element_type=jnp.float32
    ) * HEAD_DIM ** (-0.5)
    starts = offset + jnp.arange(block_count, dtype=jnp.int32) * WINDOW
    query_pos = starts[:, None] + jnp.arange(WINDOW, dtype=jnp.int32)[None, :]
    key_pos = starts[:, None] + jnp.arange(3 * WINDOW, dtype=jnp.int32)[None, :] - WINDOW
    distance = key_pos[:, None, :] - query_pos[:, :, None]
    inside = (key_pos >= 0) & (key_pos < seq_len)
    keep = (jnp.abs(distance) <= WINDOW) & inside[:, None, :]
    scores = jnp.where(keep[:, None, None], scores, masked_score)
    sink_logit = sinks.reshape(kv_local, group)[None, :, :, None, None]
    top = jnp.maximum(jnp.max(scores, axis=-1, keepdims=True), sink_logit)
    raised = jnp.exp(scores - top)
    total = jnp.sum(raised, axis=-1, keepdims=True) + jnp.exp(sink_logit - top)
    probs = (raised / total).astype(jnp.bfloat16)
    attended = jnp.einsum(
        "nkgqs,nskd->nqkgd", probs, value_band, preferred_element_type=jnp.float32
    )
    return attended.astype(jnp.bfloat16).reshape(tok_rows, query_cols)


def local(
    tokens,
    w_query,
    w_key,
    w_value,
    w_pool_in,
    sink,
    w_pool,
    pool_scale,
    w_out_attn,
    w_out_pool,
    out_gain,
):
    tok_rows = tokens.shape[0]
    seq_len = tok_rows * lax.axis_size(SP)
    offset = lax.axis_index(SP) * tok_rows
    out_both = jnp.concatenate([w_out_attn, w_out_pool], axis=0)
    out_whole = gather_axes(out_both, (("sp_0", "sp_1"), "sp_2"), 1)
    gathered = gather_directly(tokens, "tp", 1)
    key_cols = w_key.shape[1]
    chan_cols = w_pool_in.shape[1]
    query_sum, joined_sum, chan_sum = make_projector(
        gathered, side_by_side((w_query, w_key, w_value, w_pool_in), SP, 0, 1)
    )
    query = query_sum.astype(jnp.bfloat16)
    key_value = joined_sum.astype(jnp.bfloat16)
    chan = chan_sum.astype(jnp.bfloat16)
    keys_ext = padded(key_value, ((SP, 0),), WINDOW)
    attended = attend_local(query, keys_ext, sink, offset, seq_len, key_cols)
    rim_rows = 2 ** (POOL_GROUPS - 1)
    chan_ext = padded(chan, ((SP, 0),), rim_rows)
    running = jnp.concatenate(
        [jnp.zeros((1, chan_cols), jnp.float32), jnp.cumsum(chan_ext.astype(jnp.float32), axis=0)],
        axis=0,
    )
    chan_float = chan.astype(jnp.float32)
    positions = offset + jnp.arange(tok_rows, dtype=jnp.int32)
    group_count = w_pool.shape[0]
    level = lax.axis_index("tp") * group_count + 0
    half = jnp.left_shift(jnp.int32(1), level)
    upper = lax.dynamic_slice_in_dim(running, rim_rows + half, tok_rows, 0)
    lower = lax.dynamic_slice_in_dim(running, rim_rows - half, tok_rows, 0)
    count = (
        jnp.clip(positions + half, 0, seq_len) - jnp.clip(positions - half, 0, seq_len)
    ).astype(jnp.float32)
    spread = ((upper - lower) / count[:, None] - chan_float).astype(jnp.bfloat16)
    outputs = jnp.dot(spread, w_pool[0], preferred_element_type=jnp.float32)
    pooled = (outputs * pool_scale).astype(jnp.bfloat16)
    hidden = jnp.concatenate([attended, pooled], axis=1)
    terms = jnp.dot(hidden, out_whole, preferred_element_type=jnp.float32)
    share_width = out_gain.shape[0]
    model_width = share_width * lax.axis_size("tp")
    share = sent_and_summed(terms.astype(jnp.bfloat16), "tp", 1)
    row_total, row_square = in_one((jnp.sum(share, axis=1), jnp.sum(share * share, axis=1)), "tp")
    row_mean = row_total / model_width
    variance = row_square / model_width - row_mean * row_mean
    normed = (share - row_mean[:, None]) * lax.rsqrt(variance + epsilon)[:, None] * out_gain
    return normed.astype(jnp.bfloat16)


def solution(mesh):
    finer = Mesh(mesh.devices.reshape(16, 4, 2, mesh.shape["tp"]), ("sp_0", "sp_1", "sp_2", "tp"))
    return jax.shard_map(
        local,
        mesh=finer,
        in_specs=(
            P(SP, "tp"),
            P(SP, "tp"),
            P(SP, "tp"),
            P(SP, "tp"),
            P(SP, "tp"),
            P("tp"),
            P("tp", None, None),
            P("tp"),
            P("tp", SP),
            P("tp", SP),
            P("tp"),
        ),
        out_specs=P(SP, "tp"),
        check_vma=False,
    )
```

profile of v0, /device:TPU:1, one launch (start us, length us, event | category | flops | bytes accessed | tf_op | source)
XLA Modules:
  0.0 242.7 jit_solution(12594577696997631340)
XLA Ops:
  6.6 0.8 pad_maximum_fusion.3
  7.4 1.1 broadcast_in_dim.19
  8.5 19.1 %all-to-all-start.1 = ((bf16[64,512,16]{1,2,0:T(8,128)(2,1)}), bf16[64,512,16]{1,2,0:T(8,128)(2,1)S(1)}, u32[]{:S(2)}, u32[]{:S(2)}) async-start(bf16[64,512,16]{1,2,0:T(8,128)(2,1)} %broadcast_in_dim.19), calls=%async_computation.1 | async-start | bytes 2097152 | tf_op jit(solution)/shard_map/all_to_all | solution.py:19
  28.6 51.6 %all-to-all-done.1 = bf16[64,512,16]{1,2,0:T(8,128)(2,1)S(1)} async-done(((bf16[64,512,16]{1,2,0:T(8,128)(2,1)}), bf16[64,512,16]{1,2,0:T(8,128)(2,1)S(1)}, u32[]{:S(2)}, u32[]{:S(2)}) %all-to-all-start.1) | async-done | bytes 1048608 | tf_op jit(solution)/shard_map/all_to_all | solution.py:19
  80.5 10.4 %all_to_all.26 = bf16[2,64,512,16]{2,3,1,0:T(8,128)(2,1)} all-to-all(bf16[2,64,512,16]{2,3,1,0:T(8,128)(2,1)S(1)} %broadcast_in_dim.20), channel_id=1, replica_groups=mesh['sp_0'=16,'sp_1'=4,'sp_2'=2,'tp'=4] {'sp_2'}, dimensions={0} | all-to-all | bytes 4194304 | tf_op jit(solution)/shard_map/all_to_all | solution.py:19
  90.9 1.6 broadcast_in_dim.16
  92.5 4.2 %all-to-all-start = ((bf16[4,512,512]{1,2,0:T(8,128)(2,1)}), bf16[4,512,512]{1,2,0:T(8,128)(2,1)S(1)}, u32[]{:S(2)}, u32[]{:S(2)}) async-start(bf16[4,512,512]{1,2,0:T(8,128)(2,1)} %broadcast_in_dim.16), calls=%async_computation | async-start | bytes 4194304 | tf_op jit(solution)/shard_map/all_to_all | solution.py:19
  97.5 3.2 %copy.68 = bf16[2,64,512,16]{2,3,0,1:T(8,128)(2,1)} copy(bf16[2,64,512,16]{2,3,1,0:T(8,128)(2,1)} %all_to_all.26) | data formatting | bytes 4194304 | tf_op jit(solution)/shard_map/all_to_all | solution.py:19
  100.7 21.8 %all-to-all-done = bf16[4,512,512]{1,2,0:T(8,128)(2,1)S(1)} async-done(((bf16[4,512,512]{1,2,0:T(8,128)(2,1)}), bf16[4,512,512]{1,2,0:T(8,128)(2,1)S(1)}, u32[]{:S(2)}, u32[]{:S(2)}) %all-to-all-start) | async-done | bytes 2097184 | tf_op jit(solution)/shard_map/all_to_all | solution.py:19
  122.5 53.2 %all-gather.2.cloned.1.call-done = bf16[2048,640]{1,0:T(8,128)(2,1)} async-done(((bf16[16,640]{1,0:T(8,128)(2,1)}), bf16[2048,640]{1,0:T(8,128)(2,1)}) %all-gather.2.cloned.1.call-update) | async-done | bytes 2621456 | tf_op jit(solution)/shard_map/all_gather | solution.py:44
  175.7 1.7 convolution_convert_fusion.3
  177.4 2.2 collective-permute-start
  179.6 2.1 collective-permute-start.1
  181.7 0.7 fusion.9
  182.6 3.4 %collective-permute-start.2 = (bf16[8,256]{0,1:T(8,128)(2,1)S(1)}, bf16[8,256]{0,1:T(8,128)(2,1)S(1)}, u32[]{:S(2)}, u32[]{:S(2)}) collective-permute-start(bf16[8,256]{0,1:T(8,128)(2,1)S(1)} %get-tuple-element.7), channel_id=1, source_target_pairs={{0,4},{4,8},{8,12},{12,16},{16,20},{20,24},{24,28},{28,32},{32,36}... | collective-permute-start | bytes 12296 | tf_op jit(solution)/shard_map/ppermute | solution.py:59
  186.0 1.9 collective-permute-start.3
  187.9 0.7 fusion.8
  188.8 2.8 %collective-permute-done.3 = bf16[8,256]{0,1:T(8,128)(2,1)S(1)} collective-permute-done((bf16[8,256]{0,1:T(8,128)(2,1)S(1)}, bf16[8,256]{0,1:T(8,128)(2,1)S(1)}, u32[]{:S(2)}, u32[]{:S(2)}) %collective-permute-start.3) | collective-permute-done | bytes 4128 | tf_op jit(solution)/shard_map/ppermute | solution.py:61
  195.0 0.7 fusion
  195.8 0.9 fusion.10
  197.4 1.3 convolution_convert_fusion
  198.8 28.7 %all_to_all.27 = bf16[4,512,512]{2,1,0:T(8,128)(2,1)S(1)} all-to-all(bf16[4,512,512]{2,1,0:T(8,128)(2,1)S(1)} %bitcast.103), channel_id=1, replica_groups=mesh['sp_0'=16,'sp_1'=4,'sp_2'=2,'tp'=4] {'tp'}, dimensions={0} | all-to-all | bytes 4194304 | tf_op jit(solution)/shard_map/all_to_all | solution.py:76
  228.2 6.6 %all_to_all.28 = f32[4,1,1024]{2,1,0:T(1,128)S(1)} all-to-all(f32[4,1,1024]{2,1,0:T(1,128)S(1)} %broadcast_in_dim.21), channel_id=1, replica_groups=mesh['sp_0'=16,'sp_1'=4,'sp_2'=2,'tp'=4] {'tp'}, dimensions={0} | all-to-all | bytes 32768 | tf_op jit(solution)/shard_map/all_to_all | solution.py:19
  234.8 1.0 multiply_convert_fusion
  (65 shorter events, 7.0 us)
Async XLA Ops:
  6.5 186.8 %copy-start = (bf16[1,256,256]{2,1,0:T(8,128)(2,1)S(1)}, bf16[1,256,256]{2,1,0:T(8,128)(2,1)}, u32[]{:S(2)}) copy-start(bf16[1,256,256]{2,1,0:T(8,128)(2,1)} %param.17) | copy-start | bytes 393220
  6.5 21.1 %copy-start.5 = (bf16[16,256]{1,0:T(8,128)(2,1)S(1)}, bf16[16,256]{1,0:T(8,128)(2,1)}, u32[]{:S(2)}) copy-start(bf16[16,256]{1,0:T(8,128)(2,1)} %param.12) | copy-start | bytes 24580
  6.5 21.1 %copy-start.7 = (bf16[16,64]{1,0:T(8,128)(2,1)S(1)}, bf16[16,64]{1,0:T(8,128)(2,1)}, u32[]{:S(2)}) copy-start(bf16[16,64]{1,0:T(8,128)(2,1)} %param.13) | copy-start | bytes 6148
  6.5 21.1 %copy-start.6 = (bf16[16,64]{1,0:T(8,128)(2,1)S(1)}, bf16[16,64]{1,0:T(8,128)(2,1)}, u32[]{:S(2)}) copy-start(bf16[16,64]{1,0:T(8,128)(2,1)} %param.14) | copy-start | bytes 6148
  6.5 21.1 %copy-start.4 = (bf16[16,256]{1,0:T(8,128)(2,1)S(1)}, bf16[16,256]{1,0:T(8,128)(2,1)}, u32[]{:S(2)}) copy-start(bf16[16,256]{1,0:T(8,128)(2,1)} %param.15) | copy-start | bytes 24580
  6.5 21.8 %copy-start.2 = (bf16[512,512]{1,0:T(8,128)(2,1)S(1)}, bf16[512,512]{1,0:T(8,128)(2,1)}, u32[]{:S(2)}) copy-start(bf16[512,512]{1,0:T(8,128)(2,1)} %param.11) | copy-start | bytes 1572868
  8.5 71.7 %all-to-all-start.1 = ((bf16[64,512,16]{1,2,0:T(8,128)(2,1)}), bf16[64,512,16]{1,2,0:T(8,128)(2,1)S(1)}, u32[]{:S(2)}, u32[]{:S(2)}) async-start(bf16[64,512,16]{1,2,0:T(8,128)(2,1)} %broadcast_in_dim.19), calls=%async_computation.1 | async-start | bytes 2097152 | tf_op jit(solution)/shard_map/all_to_all | solution.py:19
  27.6 148.1 %all-gather.2.cloned.1.call-start = ((), (), s32[]{:S(2)}) async-start(), calls=%async_computation.5 | async-start | bytes 2641920 | tf_op jit(solution)/shard_map/all_gather | solution.py:44
  92.5 30.0 %all-to-all-start = ((bf16[4,512,512]{1,2,0:T(8,128)(2,1)}), bf16[4,512,512]{1,2,0:T(8,128)(2,1)S(1)}, u32[]{:S(2)}, u32[]{:S(2)}) async-start(bf16[4,512,512]{1,2,0:T(8,128)(2,1)} %broadcast_in_dim.16), calls=%async_computation | async-start | bytes 4194304 | tf_op jit(solution)/shard_map/all_to_all | solution.py:19
  175.7 6.0 %copy-start.3 = (bf16[2048,640]{1,0:T(8,128)(2,1)S(1)}, bf16[2048,640]{1,0:T(8,128)(2,1)}, u32[]{:S(2)}) copy-start(bf16[2048,640]{1,0:T(8,128)(2,1)} %all-gather.2.cloned.1.call-done) | copy-start | bytes 7864324
  177.4 16.7 %collective-permute-start = (bf16[128,128]{0,1:T(8,128)(2,1)S(1)}, bf16[128,128]{0,1:T(8,128)(2,1)S(1)}, u32[]{:S(2)}, u32[]{:S(2)}) collective-permute-start(bf16[128,128]{0,1:T(8,128)(2,1)S(1)} %get-tuple-element.12), channel_id=1, source_target_pairs={{0,4},{4,8},{8,12},{12,16},{16,20},{20,24},{24,28},{28,32},{32,36}... | collective-permute-start | bytes 98312 | tf_op jit(solution)/shard_map/ppermute | solution.py:59
  179.6 14.5 %collective-permute-start.1 = (bf16[128,128]{0,1:T(8,128)(2,1)S(1)}, bf16[128,128]{0,1:T(8,128)(2,1)S(1)}, u32[]{:S(2)}, u32[]{:S(2)}) collective-permute-start(bf16[128,128]{0,1:T(8,128)(2,1)S(1)} %get-tuple-element.11), channel_id=1, source_target_pairs={{4,0},{8,4},{12,8},{16,12},{20,16},{24,20},{28,24},{32,28},{36,32}... | collective-permute-start | bytes 98312 | tf_op jit(solution)/shard_map/ppermute | solution.py:61
  182.6 6.2 %collective-permute-start.2 = (bf16[8,256]{0,1:T(8,128)(2,1)S(1)}, bf16[8,256]{0,1:T(8,128)(2,1)S(1)}, u32[]{:S(2)}, u32[]{:S(2)}) collective-permute-start(bf16[8,256]{0,1:T(8,128)(2,1)S(1)} %get-tuple-element.7), channel_id=1, source_target_pairs={{0,4},{4,8},{8,12},{12,16},{16,20},{20,24},{24,28},{28,32},{32,36}... | collective-permute-start | bytes 12296 | tf_op jit(solution)/shard_map/ppermute | solution.py:59
  186.0 5.6 %collective-permute-start.3 = (bf16[8,256]{0,1:T(8,128)(2,1)S(1)}, bf16[8,256]{0,1:T(8,128)(2,1)S(1)}, u32[]{:S(2)}, u32[]{:S(2)}) collective-permute-start(bf16[8,256]{0,1:T(8,128)(2,1)S(1)} %get-tuple-element.8), channel_id=1, source_target_pairs={{4,0},{8,4},{12,8},{16,12},{20,16},{24,20},{28,24},{32,28},{36,32}... | collective-permute-start | bytes 12296 | tf_op jit(solution)/shard_map/ppermute | solution.py:61
  192.8 0.7 copy-start.10
  194.1 0.9 copy-start.9
  195.8 1.6 copy-start.1
  227.5 7.3 %copy-start.8 = (f32[512]{0:T(512)S(1)}, f32[512]{0:T(512)}, u32[]{:S(2)}) copy-start(f32[512]{0:T(512)} %param.21) | copy-start | bytes 6148
Sparse Core Ops, SparseCore 0:
  31.4 144.2 all-gather.1
where the time goes:
time: 245 us; the launch traced here: 243 us
  waiting for transfers between devices  129 us (53%)
  blocking collectives  45.7 us (19%)
  starting transfers between devices  33 us (13%)
  between operations  13.8 us (6%)
  local copies, waits for them, and re-layouts  8.25 us (3%)
  matrix products  6.59 us (3%)
  other arithmetic  5.83 us (2%)
    all_to_all x2, waiting for transfers between devices, from_everyone(): lax.all_to_all(jnp.broadcast_to(shard[None], (count, *shard.shape)), axis...  73.4 us
    all_gather x1, waiting for transfers between devices, side_by_side(): lax.all_gather(both, axis, axis=dim, tiled=True)  53.2 us
    all_to_all x1, blocking collectives, sent_and_summed(): lax.all_to_all(cut_along(shard, dim, count), axis, 0, 0, tiled=True)  28.7 us
    all_to_all x2, starting transfers between devices, from_everyone(): lax.all_to_all(jnp.broadcast_to(shard[None], (count, *shard.shape)), axis...  23.3 us
    all_to_all x2, blocking collectives, from_everyone(): lax.all_to_all(jnp.broadcast_to(shard[None], (count, *shard.shape)), axis...  17 us
    ppermute x2, starting transfers between devices, padded(): lax.ppermute(tail, axis, [(i, (i + 1) % count) for i in range(ends)])  5.65 us
  transfers between devices with their start and end apart: 7, of which 4 were waited for; matrix products, arithmetic and copies ran while one was open for 4% of the time, Pallas kernels for 0%

commit v1 on v0

v1 whole, which is shorter than its diff:
```python
import jax
import jax.numpy as jnp
from jax import lax
from jax.experimental import pallas as pl
from jax.experimental.pallas import tpu as pltpu
from jax.sharding import Mesh
from jax.sharding import PartitionSpec as P

HEAD_DIM = 64
WINDOW = 128
RIM = 16
SP = ("sp_0", "sp_1", "sp_2")
MESH = pl.DeviceIdType.MESH
NZ, NX, NC, NY = 16, 4, 2, 4

epsilon = 1e-05
masked_score = -1e30

BATCHES = ((0, 5), (12, 16), (5, 8), (8, 12))
NT = (((1,), (1,)), ((), ()))
BF16, F32 = jnp.bfloat16, jnp.float32


def kernel(
    tok_hbm, wq_ref, wk_ref, wv_ref, wc_ref, sink_ref, wpool_ref, scale_ref, woa_ref, wop_ref, gain_ref,
    out_hbm,
    toks, win, wout, win_abs, wout_abs, query, kv, chan, hid, part, comb, relayed, from_prev, from_next,
    share, stats, outv, local_sem, out_sem, send_sem, recv_sem,
):
    z, x, c, y = (lax.axis_index(a) for a in (*SP, "tp"))
    rows, feats = toks.shape[1], toks.shape[2]
    seq_len = rows * NZ * NX * NC
    blocks = rows // WINDOW
    place = (z * NX + x) * NC + c
    offset = place * rows
    total_places = NZ * NX * NC

    def dev_z(d):
        return {"sp_0": lax.rem(z + (d + NZ), NZ)}

    def dev_x(d):
        return {"sp_1": lax.rem(x + (d + NX), NX)}

    def dev_y(d):
        return {"tp": lax.rem(y + (d + NY), NY)}

    dev_c = {"sp_2": 1 - c}

    def dev_sp(d):
        s = lax.rem(place + (d + total_places), total_places)
        return {
            "sp_0": lax.div(s, NX * NC),
            "sp_1": lax.rem(lax.div(s, NC), NX),
            "sp_2": lax.rem(s, NC),
        }

    peers = [dev_z(d) for d in (1, -1, 2, -2, 3, -3, 4, -4)]
    peers += [dev_x(1), dev_x(-1), dev_c, dev_y(1), dev_y(-1), dev_y(2), dev_sp(1), dev_sp(-1)]

    own_tokens = pltpu.make_async_copy(tok_hbm, toks.at[0], local_sem)
    own_tokens.start()
    barrier = pltpu.get_barrier_semaphore()
    for peer in peers:
        pl.semaphore_signal(barrier, inc=1, device_id=peer, device_id_type=MESH)

    win[0, 0, 0, :, 0:256] = wq_ref[...]
    win[0, 0, 0, :, 256:384] = jnp.concatenate([wk_ref[...], wv_ref[...]], axis=1)
    win[0, 0, 0, :, 384:640] = wc_ref[...]
    eye = jnp.where(
        lax.broadcasted_iota(jnp.int32, (16, 16), 0) == lax.broadcasted_iota(jnp.int32, (16, 16), 1), 1.0, 0.0
    ).astype(BF16)
    wout[0, 0, 0, :, 0:256] = lax.dot_general(eye, woa_ref[...], NT, preferred_element_type=F32).astype(BF16)
    wout[0, 0, 0, :, 256:512] = lax.dot_general(eye, wop_ref[...], NT, preferred_element_type=F32).astype(BF16)

    own_tokens.wait()
    pl.semaphore_wait(barrier, len(peers))

    used = []

    def message(src, dst, device):
        m = len(used)
        copy = pltpu.make_async_remote_copy(
            src_ref=src, dst_ref=dst, send_sem=send_sem.at[m], recv_sem=recv_sem.at[m],
            device_id=device, device_id_type=MESH,
        )
        used.append(copy)
        return copy

    class Gather:
        def __init__(self, w):
            self.w = w
            self.slot = {}
            for d in (4, -4, 3, -3, 2, -2, 1, -1):
                self.slot[(-d) % NZ] = message(w.at[0, 0, 0], w.at[0, 0, (-d) % NZ], dev_z(d))
            for e in (4, 3, 2, 1):
                self.slot[12 - e] = message(w.at[0, 0, 12], w.at[0, 0, 12 - e], dev_z(e))
            for e in (3, 2, 1):
                self.slot[4 + e] = message(w.at[0, 0, 4], w.at[0, 0, 4 + e], dev_z(-e))
            self.xp, self.xm, self.xr, self.cc = [], [], [], {}
            for b, (lo, hi) in enumerate(BATCHES):
                at = pl.ds(lo, hi - lo)
                self.xp.append(message(w.at[0, 0, at], w.at[3, 0, at], dev_x(1)))
                self.xm.append(message(w.at[0, 0, at], w.at[1, 0, at], dev_x(-1)))
                if b % 2 == 0:
                    self.xr.append(message(w.at[3, 0, at], w.at[2, 0, at], dev_x(1)))
                else:
                    self.xr.append(message(w.at[1, 0, at], w.at[2, 0, at], dev_x(-1)))
                for r in range(NX):
                    self.cc[r, b] = message(w.at[r, 0, at], w.at[r, 1, at], dev_c)

        def near(self):
            for d in (4, -4, 3, -3, 2, -2, 1, -1):
                self.slot[(-d) % NZ].start()

        def far(self):
            self.slot[12].wait_recv()
            for e in (4, 3, 2, 1):
                self.slot[12 - e].start()
            self.slot[4].wait_recv()
            for e in (3, 2, 1):
                self.slot[4 + e].start()

        def along_x(self, b):
            lo, hi = BATCHES[b]
            for s in range(lo, hi):
                if s not in (0, 4, 12):
                    self.slot[s].wait_recv()
            self.xp[b].start()
            self.xm[b].start()
            self.cc[0, b].start()

        def relay_x(self, b):
            self.xp[b].wait_recv()
            if b % 2 == 0:
                self.xr[b].start()
            self.cc[3, b].start()
            self.xm[b].wait_recv()
            if b % 2 == 1:
                self.xr[b].start()
            self.cc[1, b].start()

        def last_x(self, b):
            self.xr[b].wait_recv()
            self.cc[2, b].start()

        def done(self):
            for b in range(len(BATCHES)):
                for r in (0, 3, 1, 2):
                    self.cc[r, b].wait_recv()

        def in_order(self, dest):
            w = self.w

            def one(j, carry):
                base = lax.rem(z + j, NZ) * (NX * NC * 16)
                for r in range(NX):
                    for k in range(NC):
                        at = base + lax.rem(x + r, NX) * (NC * 16) + lax.rem(c + k, NC) * 16
                        dest[pl.ds(pl.multiple_of(at, 16), 16), :] = w[r, k, j]
                return carry

            lax.fori_loop(0, NZ, one, 0)

    into = Gather(win)
    outof = Gather(wout)

    def chunk(b):
        return pl.ds(b * WINDOW, WINDOW)

    tok_plus = [message(toks.at[0, chunk(b)], toks.at[3, chunk(b)], dev_y(1)) for b in range(4)]
    tok_minus = [message(toks.at[0, chunk(b)], toks.at[1, chunk(b)], dev_y(-1)) for b in range(4)]
    tok_relay = [
        message(toks.at[3, chunk(b)], toks.at[2, chunk(b)], dev_y(1)) if b < 2
        else message(toks.at[1, chunk(b)], toks.at[2, chunk(b)], dev_y(-1))
        for b in range(4)
    ]

    into.near()
    for b in (0, 1):
        tok_plus[b].start()
        tok_minus[b + 2].start()
    for b in (0, 1):
        tok_plus[b + 2].start()
        tok_minus[b].start()
    into.far()
    outof.near()
    tok_plus[0].wait_recv()
    tok_relay[0].start()
    tok_minus[2].wait_recv()
    tok_relay[2].start()
    into.along_x(0)
    into.along_x(1)
    outof.far()
    tok_plus[1].wait_recv()
    tok_relay[1].start()
    tok_minus[3].wait_recv()
    tok_relay[3].start()
    into.along_x(2)
    into.along_x(3)
    for b in range(4):
        into.relay_x(b)
    for b in range(4):
        into.last_x(b)
    outof.along_x(0)
    outof.along_x(1)
    into.done()
    into.in_order(win_abs)
    outof.along_x(2)
    outof.along_x(3)
    for b in (2, 3):
        tok_plus[b].wait_recv()
        tok_minus[b - 2].wait_recv()
    for b in range(4):
        tok_relay[b].wait_recv()

    for m in range(2):
        at = pl.ds(m * 256, 256)
        for lo, hi in ((256, 384), (384, 640), (0, 256)):
            acc = jnp.zeros((256, hi - lo), F32)
            for r in range(NY):
                depth = pl.ds(pl.multiple_of(lax.rem(y + r, NY) * feats, feats), feats)
                acc = acc + jnp.dot(toks[r, at, :], win_abs[depth, lo:hi], preferred_element_type=F32)
            if lo == 256:
                kv[pl.ds(WINDOW + m * 256, 256), :] = acc.astype(BF16)
            elif lo == 384:
                chan[pl.ds(RIM + m * 256, 256), :] = acc.astype(BF16)
            else:
                query[at, :] = (acc * HEAD_DIM ** (-0.5)).astype(BF16)

    kv_next = message(kv.at[pl.ds(rows, WINDOW)], kv.at[pl.ds(0, WINDOW)], dev_sp(1))
    kv_prev = message(kv.at[pl.ds(WINDOW, WINDOW)], kv.at[pl.ds(WINDOW + rows, WINDOW)], dev_sp(-1))
    ch_next = message(chan.at[pl.ds(rows, RIM)], chan.at[pl.ds(0, RIM)], dev_sp(1))
    ch_prev = message(chan.at[pl.ds(RIM, RIM)], chan.at[pl.ds(RIM + rows, RIM)], dev_sp(-1))
    for copy in (kv_next, kv_prev, ch_next, ch_prev):
        copy.start()

    for b in range(4):
        outof.relay_x(b)
    for b in range(4):
        outof.last_x(b)

    half = lax.shift_left(jnp.int32(1), y.astype(jnp.int32))

    def mixers(n):
        at = pl.ds(n * WINDOW, WINDOW)
        first = offset + n * WINDOW
        i = lax.broadcasted_iota(jnp.int32, (WINDOW, 3 * WINDOW), 0)
        j = lax.broadcasted_iota(jnp.int32, (WINDOW, 3 * WINDOW), 1)
        pos = first + j - WINDOW
        keep = (j >= i) & (j <= i + 2 * WINDOW) & (pos >= 0) & (pos < seq_len)
        band = kv[pl.ds(n * WINDOW, 3 * WINDOW), :]
        keys, values = band[:, :HEAD_DIM], band[:, HEAD_DIM:]
        heads = []
        for h in range(4):
            q = query[at, h * HEAD_DIM : (h + 1) * HEAD_DIM]
            scores = lax.dot_general(q, keys, NT, preferred_element_type=F32)
            scores = jnp.where(keep, scores, masked_score)
            sink = sink_ref[h]
            top = jnp.maximum(jnp.max(scores, axis=1, keepdims=True), sink)
            raised = jnp.exp(scores - top)
            total = jnp.sum(raised, axis=1, keepdims=True) + jnp.exp(sink - top)
            probs = (raised * (1.0 / total)).astype(BF16)
            heads.append(jnp.dot(probs, values, preferred_element_type=F32).astype(BF16))
        hid[at, 0:256] = jnp.concatenate(heads, axis=1)

        i = lax.broadcasted_iota(jnp.int32, (WINDOW, WINDOW + 2 * RIM), 0)
        j = lax.broadcasted_iota(jnp.int32, (WINDOW, WINDOW + 2 * RIM), 1) - RIM
        pos = first + j
        member = (j >= i - half) & (j < i + half) & (pos >= 0) & (pos < seq_len)
        member = jnp.where(member, 1.0, 0.0).astype(BF16)
        sums = jnp.dot(member, chan[pl.ds(n * WINDOW, WINDOW + 2 * RIM), :], preferred_element_type=F32)
        t = first + lax.broadcasted_iota(jnp.int32, (WINDOW, 1), 0)
        count = (jnp.minimum(t + half, seq_len) - jnp.maximum(t - half, 0)).astype(F32)
        spread = (sums / count - chan[pl.ds(n * WINDOW + RIM, WINDOW), :].astype(F32)).astype(BF16)
        pooled = jnp.dot(spread, wpool_ref[0], preferred_element_type=F32) * scale_ref[...]
        hid[at, 256:512] = pooled.astype(BF16)

    def partials(n):
        at = pl.ds(n * WINDOW, WINDOW)
        for d in (2, 1, 3, 0):
            cols = pl.ds(pl.multiple_of(lax.rem(y + d, NY) * feats, feats), feats)
            terms = lax.dot_general(hid[at, :], wout_abs[cols, :], NT, preferred_element_type=F32)
            part[d, at, :] = terms.astype(BF16)

    via, straight, joined = {}, {}, {}
    for n in range(4):
        at = chunk(n)
        if n < 2:
            via[n] = message(part.at[2, at], relayed.at[at], dev_y(1))
            straight[n] = message(part.at[3, at], from_next.at[at], dev_y(-1))
            joined[n] = message(comb.at[at], from_prev.at[at], dev_y(1))
        else:
            via[n] = message(part.at[2, at], relayed.at[at], dev_y(-1))
            straight[n] = message(part.at[1, at], from_prev.at[at], dev_y(1))
            joined[n] = message(comb.at[at], from_next.at[at], dev_y(-1))

    def send(n):
        via[n].start()
        straight[n].start()

    def relay(n):
        at = chunk(n)
        via[n].wait_recv()
        mine = part[1 if n < 2 else 3, at, :]
        comb[at, :] = (mine.astype(F32) + relayed[at, :].astype(F32)).astype(BF16)
        joined[n].start()

    mixers(1)
    mixers(2)
    outof.done()
    outof.in_order(wout_abs)
    partials(1)
    send(1)
    partials(2)
    send(2)
    kv_next.wait_recv()
    ch_next.wait_recv()
    mixers(0)
    partials(0)
    send(0)
    kv_prev.wait_recv()
    ch_prev.wait_recv()
    mixers(3)
    relay(1)
    relay(2)
    partials(3)
    send(3)
    relay(0)
    relay(3)

    lane = lax.broadcasted_iota(jnp.int32, (WINDOW, 128), 1)
    for n in (1, 2, 0, 3):
        at = chunk(n)
        straight[n].wait_recv()
        joined[n].wait_recv()
        mix = part[0, at, :].astype(F32) + from_prev[at, :].astype(F32) + from_next[at, :].astype(F32)
        share[at, :] = mix
        one = jnp.sum(mix, axis=1, keepdims=True)
        two = jnp.sum(mix * mix, axis=1, keepdims=True)
        both = jnp.where(lane == 0, one, jnp.where(lane == 1, two, 0.0))
        stats[0, n * 8 : n * 8 + 8, :] = both.T[0:8]

    told = [
        message(stats.at[0], stats.at[3], dev_y(1)),
        message(stats.at[0], stats.at[1], dev_y(-1)),
        message(stats.at[0], stats.at[2], dev_y(2)),
    ]
    for copy in told:
        copy.start()
    for copy in told:
        copy.wait_recv()
    width = feats * NY
    writes = []
    for n in range(4):
        at = chunk(n)
        eight = slice(n * 8, n * 8 + 8)
        both = stats[0, eight, :] + stats[1, eight, :] + stats[2, eight, :] + stats[3, eight, :]
        both = jnp.concatenate([both] * 16, axis=0).T
        mean = both[:, 0:1] / width
        variance = both[:, 1:2] / width - mean * mean
        normed = (share[at, :] - mean) * lax.rsqrt(variance + epsilon) * gain_ref[...]
        outv[at, :] = normed.astype(BF16)
        write = pltpu.make_async_copy(outv.at[at], out_hbm.at[at], out_sem.at[n])
        write.start()
        writes.append(write)
    for copy in used:
        copy.wait_send()
    for write in writes:
        write.wait()


MESSAGES = 2 * (15 + 12 + 16) + 12 + 4 + 12 + 3


def local(tokens, w_query, w_key, w_value, w_pool_in, sink, w_pool, pool_scale, w_out_attn, w_out_pool, out_gain):
    rows, feats = tokens.shape
    vmem = pl.BlockSpec(memory_space=pltpu.VMEM)
    smem = pl.BlockSpec(memory_space=pltpu.SMEM)
    hbm = pl.BlockSpec(memory_space=pl.ANY)
    lanes_in = 640
    lanes_out = 512
    model = feats * NY
    return pl.pallas_call(
        kernel,
        out_shape=jax.ShapeDtypeStruct((rows, feats), BF16),
        in_specs=[hbm, vmem, vmem, vmem, vmem, smem, vmem, vmem, vmem, vmem, vmem],
        out_specs=hbm,
        scratch_shapes=[
            pltpu.VMEM((NY, rows, feats), BF16),
            pltpu.VMEM((NX, NC, NZ, 16, lanes_in), BF16),
            pltpu.VMEM((NX, NC, NZ, 16, lanes_out), BF16),
            pltpu.VMEM((model, lanes_in), BF16),
            pltpu.VMEM((model, lanes_out), BF16),
            pltpu.VMEM((rows, 256), BF16),
            pltpu.VMEM((rows + 2 * WINDOW, 128), BF16),
            pltpu.VMEM((rows + 2 * RIM, 256), BF16),
            pltpu.VMEM((rows, lanes_out), BF16),
            pltpu.VMEM((NY, rows, feats), BF16),
            pltpu.VMEM((rows, feats), BF16),
            pltpu.VMEM((rows, feats), BF16),
            pltpu.VMEM((rows, feats), BF16),
            pltpu.VMEM((rows, feats), BF16),
            pltpu.VMEM((rows, feats), F32),
            pltpu.VMEM((NY, 32, 128), F32),
            pltpu.VMEM((rows, feats), BF16),
            pltpu.SemaphoreType.DMA,
            pltpu.SemaphoreType.DMA((4,)),
            pltpu.SemaphoreType.DMA((MESSAGES,)),
            pltpu.SemaphoreType.DMA((MESSAGES,)),
        ],
        compiler_params=pltpu.CompilerParams(collective_id=0, has_side_effects=True),
    )(
        tokens, w_query, w_key, w_value, w_pool_in, sink, w_pool, pool_scale.reshape(1, -1),
        w_out_attn, w_out_pool, out_gain.reshape(1, -1),
    )


def solution(mesh):
    finer = Mesh(mesh.devices.reshape(NZ, NX, NC, NY), (*SP, "tp"))
    return jax.shard_map(
        local,
        mesh=finer,
        in_specs=(
            P(SP, "tp"), P(SP, "tp"), P(SP, "tp"), P(SP, "tp"), P(SP, "tp"), P("tp"),
            P("tp", None, None), P("tp"), P("tp", SP), P("tp", SP), P("tp"),
        ),
        out_specs=P(SP, "tp"),
        check_vma=False,
    )
```

time: 245 us -> 85.3 us (0.35)
  the two profiles are of different devices: /device:TPU:1 before, /device:TPU:32 now
where the time goes in v1:
time: 85.3 us; the launch traced here: 85.1 us
  Pallas kernels  81 us (95%)
  local copies, waits for them, and re-layouts  4.06 us (5%)
    pallas_call x1, Pallas kernels, local(): pl.pallas_call(kernel, out_shape=jax.ShapeDtypeStruct((rows, feats), BF16...  81 us
    unnamed x5, local copies, waits for them, and re-layouts  4.06 us

profile of v1, /device:TPU:32, one launch (start us, length us, event | category | flops | bytes accessed | tf_op | source)
XLA Modules:
  0.0 85.1 jit_solution(15482340992100801842)
XLA Ops:
  0.0 0.0 copy-start
  0.0 1.4 %copy.12.woa_ref = bf16[256,16]{1,0:T(8,128)(2,1)} copy(bf16[256,16]{0,1:T(8,128)(2,1)} %param.19) | data formatting | bytes 16384 | tf_op args[8]
  1.4 0.0 copy-done
  1.4 0.7 copy.13.wop_ref
  2.2 81.0 %shard_map.109 = bf16[512,512]{1,0:T(8,128)(2,1)} custom-call(bf16[512,512]{1,0:T(8,128)(2,1)} %tok_hbm.1, bf16[16,256]{1,0:T(8,128)(2,1)} %wq_ref.1, bf16[16,64]{1,0:T(8,128)(2,1)} %wk_ref.1, bf16[16,64]{1,0:T(8,128)(2,1)} %wv_ref.1, bf16[16,256]{1,0:T(8,128)(2,1)} %wc_ref.1, f32[4]{0:T(128)} %sink_ref.1, bf16[1,256,256]{2,1,0:T(8,128)(2,1)} %wpool_ref.1, ...), custom_call_target="tpu_custom_call" | custom-call | tf_op jit(solution)/shard_map/pallas_call | solution.py:383
  83.2 1.9 %copy.15 = bf16[512,512]{1,0:T(8,128)(2,1)} copy(bf16[512,512]{1,0:T(8,128)(2,1)} %shard_map.109) | data formatting | bytes 1048576
Async XLA Ops:
  0.0 1.4 %copy-start = (bf16[256,16]{0,1:T(8,128)(2,1)S(1)}, bf16[256,16]{0,1:T(8,128)(2,1)}, u32[]{:S(2)}) copy-start(bf16[256,16]{0,1:T(8,128)(2,1)} %param.20) | copy-start | bytes 24580

commit v2 on v1

v2 whole, which is shorter than its diff:
```python
import jax
import jax.numpy as jnp
from jax import lax
from jax.experimental import pallas as pl
from jax.experimental.pallas import tpu as pltpu
from jax.sharding import Mesh
from jax.sharding import PartitionSpec as P

HEAD_DIM = 64
WINDOW = 128
RIM = 16
SP = ("sp_0", "sp_1", "sp_2")
MESH = pl.DeviceIdType.MESH
NZ, NX, NC, NY = 16, 4, 2, 4

epsilon = 1e-05
masked_score = -1e30

BATCHES = ((0, 1), (1, 5), (12, 16), (5, 8), (8, 12))
OWN, NEAR_A, NEAR_B, FAR_A, FAR_B = range(5)
NT = (((1,), (1,)), ((), ()))
TN = (((0,), (0,)), ((), ()))
BF16, F32 = jnp.bfloat16, jnp.float32


def kernel(
    tok_hbm, wq_hbm, wk_hbm, wv_hbm, wc_hbm, sink_hbm, wpool_hbm, scale_hbm, woa_hbm, wop_hbm, gain_hbm,
    out_hbm,
    toks, win, wout, win_abs, wout_abs, query, kv, chan, hid, part, comb, relayed, from_prev, from_next,
    share, stats, wk, wv, sink, wpool, scale, gain, outv, local_sem, out_sem, send_sem, recv_sem,
):
    z, x, c, y = (lax.axis_index(a) for a in (*SP, "tp"))
    rows, feats = toks.shape[1], toks.shape[2]
    seq_len = rows * NZ * NX * NC
    place = (z * NX + x) * NC + c
    offset = place * rows
    total_places = NZ * NX * NC

    def dev_z(d):
        return {"sp_0": lax.rem(z + (d + NZ), NZ)}

    def dev_x(d):
        return {"sp_1": lax.rem(x + (d + NX), NX)}

    def dev_y(d):
        return {"tp": lax.rem(y + (d + NY), NY)}

    dev_c = {"sp_2": 1 - c}

    def dev_sp(d):
        s = lax.rem(place + (d + total_places), total_places)
        return {
            "sp_0": lax.div(s, NX * NC),
            "sp_1": lax.rem(lax.div(s, NC), NX),
            "sp_2": lax.rem(s, NC),
        }

    peers = [dev_z(d) for d in (4, -4, 3, -3, 2, -2, 1, -1)]
    peers += [dev_y(2), dev_x(2), dev_sp(1), dev_sp(-1), dev_x(1), dev_x(-1), dev_y(1), dev_y(-1), dev_c]
    barrier = pltpu.get_barrier_semaphore()
    for peer in peers:
        pl.semaphore_signal(barrier, inc=1, device_id=peer, device_id_type=MESH)

    mine_in, mine_out = win.at[0, 0, 0], wout.at[0, 0, 0]
    pairs = (
        (wk_hbm, wk), (wv_hbm, wv), (wq_hbm, mine_in.at[:, pl.ds(0, 256)]), (wc_hbm, mine_in.at[:, pl.ds(384, 256)]),
        (tok_hbm, toks.at[0]), (woa_hbm, mine_out.at[:, pl.ds(0, 256)]), (wop_hbm, mine_out.at[:, pl.ds(256, 256)]),
        (wpool_hbm, wpool), (scale_hbm, scale), (gain_hbm, gain), (sink_hbm, sink),
    )
    loads = [pltpu.make_async_copy(a, b, local_sem.at[k]) for k, (a, b) in enumerate(pairs)]
    for load in loads:
        load.start()

    with jax.named_scope("entry"):
        loads[0].wait()
        loads[1].wait()
        win[0, 0, 0, :, 256:384] = jnp.concatenate([wk[...], wv[...]], axis=1)
        for load in loads[2:]:
            load.wait()
        pl.semaphore_wait(barrier, len(peers))

    used = []

    def message(src, dst, device):
        m = len(used)
        copy = pltpu.make_async_remote_copy(
            src_ref=src, dst_ref=dst, send_sem=send_sem.at[m], recv_sem=recv_sem.at[m],
            device_id=device, device_id_type=MESH,
        )
        used.append(copy)
        return copy

    class Gather:
        def __init__(self, w):
            self.w = w
            self.slot = {}
            for d in (4, -4, 3, -3, 2, -2, 1, -1):
                self.slot[(-d) % NZ] = message(w.at[0, 0, 0], w.at[0, 0, (-d) % NZ], dev_z(d))
            for e in (4, 3, 2, 1):
                self.slot[12 - e] = message(w.at[0, 0, 12], w.at[0, 0, 12 - e], dev_z(e))
            for e in (3, 2, 1):
                self.slot[4 + e] = message(w.at[0, 0, 4], w.at[0, 0, 4 + e], dev_z(-e))
            self.xp, self.xm, self.xr, self.cc = [], [], [], {}
            for b, (lo, hi) in enumerate(BATCHES):
                at = pl.ds(lo, hi - lo)
                self.xp.append(message(w.at[0, 0, at], w.at[3, 0, at], dev_x(1)))
                self.xm.append(message(w.at[0, 0, at], w.at[1, 0, at], dev_x(-1)))
                if b == OWN:
                    self.xr.append(message(w.at[0, 0, at], w.at[2, 0, at], dev_x(2)))
                elif b in (NEAR_A, FAR_A):
                    self.xr.append(message(w.at[3, 0, at], w.at[2, 0, at], dev_x(1)))
                else:
                    self.xr.append(message(w.at[1, 0, at], w.at[2, 0, at], dev_x(-1)))
                for r in range(NX):
                    self.cc[r, b] = message(w.at[r, 0, at], w.at[r, 1, at], dev_c)

        def near(self):
            for d in (4, -4, 3, -3, 2, -2, 1, -1):
                self.slot[(-d) % NZ].start()

        def own(self):
            self.xp[OWN].start()
            self.xm[OWN].start()
            self.xr[OWN].start()
            self.cc[0, OWN].start()

        def far(self):
            self.slot[12].wait_recv()
            for e in (4, 3, 2, 1):
                self.slot[12 - e].start()
            self.slot[4].wait_recv()
            for e in (3, 2, 1):
                self.slot[4 + e].start()

        def along_x(self, b):
            lo, hi = BATCHES[b]
            for s in range(lo, hi):
                if s not in (4, 12):
                    self.slot[s].wait_recv()
            self.xp[b].start()
            self.xm[b].start()
            self.cc[0, b].start()

        def relay_x(self, b):
            self.xp[b].wait_recv()
            if b in (NEAR_A, FAR_A):
                self.xr[b].start()
            self.cc[3, b].start()
            self.xm[b].wait_recv()
            if b in (NEAR_B, FAR_B):
                self.xr[b].start()
            self.cc[1, b].start()

        def last_x(self, b):
            self.xr[b].wait_recv()
            self.cc[2, b].start()

        def in_order(self, dest, b):
            w = self.w
            for r in (0, 3, 1, 2):
                self.cc[r, b].wait_recv()

            def one(j, carry):
                base = lax.rem(z + j, NZ) * (NX * NC * 16)
                for r in range(NX):
                    for k in range(NC):
                        at = base + lax.rem(x + r, NX) * (NC * 16) + lax.rem(c + k, NC) * 16
                        dest[pl.ds(pl.multiple_of(at, 16), 16), :] = w[r, k, j]
                return carry

            lax.fori_loop(*BATCHES[b], one, 0)

    into = Gather(win)
    outof = Gather(wout)

    def chunk(b):
        return pl.ds(b * WINDOW, WINDOW)

    tok_plus = [message(toks.at[0, chunk(b)], toks.at[3, chunk(b)], dev_y(1)) for b in range(4)]
    tok_minus = [message(toks.at[0, chunk(b)], toks.at[1, chunk(b)], dev_y(-1)) for b in range(4)]
    tok_relay = [
        message(toks.at[3, chunk(b)], toks.at[2, chunk(b)], dev_y(1)) if b < 2
        else message(toks.at[1, chunk(b)], toks.at[2, chunk(b)], dev_y(-1))
        for b in range(4)
    ]

    with jax.named_scope("near"):
        into.near()
        into.own()
        for b in (0, 1):
            tok_plus[b].start()
            tok_minus[b + 2].start()
        for b in (0, 1):
            tok_plus[b + 2].start()
            tok_minus[b].start()
    with jax.named_scope("in_far"):
        into.far()
        outof.near()
    with jax.named_scope("in_x_near"):
        into.along_x(NEAR_A)
        into.along_x(NEAR_B)
        outof.own()
    with jax.named_scope("tok_relay_a"):
        tok_plus[0].wait_recv()
        tok_relay[0].start()
        tok_minus[2].wait_recv()
        tok_relay[2].start()
        into.relay_x(OWN)
        into.last_x(OWN)
    with jax.named_scope("in_x_relay_near"):
        into.relay_x(NEAR_A)
        into.relay_x(NEAR_B)
    with jax.named_scope("tok_relay_b"):
        tok_plus[1].wait_recv()
        tok_relay[1].start()
        tok_minus[3].wait_recv()
        tok_relay[3].start()
    with jax.named_scope("in_x_far"):
        into.along_x(FAR_A)
        into.along_x(FAR_B)
        outof.relay_x(OWN)
        outof.last_x(OWN)
    with jax.named_scope("out_far"):
        outof.far()
    with jax.named_scope("in_x_relay_far"):
        into.relay_x(FAR_A)
        into.relay_x(FAR_B)
    with jax.named_scope("out_x_near"):
        outof.along_x(NEAR_A)
        outof.along_x(NEAR_B)
    with jax.named_scope("in_last"):
        for b in (NEAR_A, NEAR_B):
            into.last_x(b)
        for b in (OWN, NEAR_A, NEAR_B):
            into.in_order(win_abs, b)
        for b in (FAR_A, FAR_B):
            into.last_x(b)
    with jax.named_scope("out_x_relay_near"):
        outof.relay_x(NEAR_A)
        outof.relay_x(NEAR_B)
    with jax.named_scope("in_order"):
        for b in (FAR_A, FAR_B):
            into.in_order(win_abs, b)
    with jax.named_scope("tok_done"):
        for b in (2, 3):
            tok_plus[b].wait_recv()
            tok_minus[b - 2].wait_recv()
        for b in range(4):
            tok_relay[b].wait_recv()

    with jax.named_scope("project"):
        for lo, hi in ((256, 384), (384, 640), (0, 256)):
            acc = jnp.zeros((rows, hi - lo), F32)
            for r in range(NY):
                depth = pl.ds(pl.multiple_of(lax.rem(y + r, NY) * feats, feats), feats)
                acc = acc + jnp.dot(toks[r], win_abs[depth, lo:hi], preferred_element_type=F32)
            if lo == 256:
                kv[pl.ds(WINDOW, rows), :] = acc.astype(BF16)
            elif lo == 384:
                chan[pl.ds(RIM, rows), :] = acc.astype(BF16)
            else:
                query[...] = (acc * HEAD_DIM ** (-0.5)).astype(BF16)

    kv_next = message(kv.at[pl.ds(rows, WINDOW)], kv.at[pl.ds(0, WINDOW)], dev_sp(1))
    kv_prev = message(kv.at[pl.ds(WINDOW, WINDOW)], kv.at[pl.ds(WINDOW + rows, WINDOW)], dev_sp(-1))
    ch_next = message(chan.at[pl.ds(rows, RIM)], chan.at[pl.ds(0, RIM)], dev_sp(1))
    ch_prev = message(chan.at[pl.ds(RIM, RIM)], chan.at[pl.ds(RIM + rows, RIM)], dev_sp(-1))
    halos = (kv_next, kv_prev, ch_next, ch_prev)
    for copy in halos:
        copy.start()

    with jax.named_scope("out_x_far"):
        outof.along_x(FAR_A)
        outof.along_x(FAR_B)

    half = lax.shift_left(jnp.int32(1), y.astype(jnp.int32))
    sinks = jnp.concatenate([jnp.broadcast_to(sink[0:1, h : h + 1], (1, WINDOW)) for h in range(4)], axis=1)

    def attend(n):
        first = offset + n * WINDOW
        band = kv[pl.ds(n * WINDOW, 3 * WINDOW), :]
        keys, values = band[:, :HEAD_DIM], band[:, HEAD_DIM:]
        block = query[n * WINDOW : (n + 1) * WINDOW, :]
        stacked = jnp.concatenate([block[:, h * HEAD_DIM : (h + 1) * HEAD_DIM] for h in range(4)], axis=0)
        scores = lax.dot_general(keys, stacked, NT, preferred_element_type=F32)
        j = lax.broadcasted_iota(jnp.int32, (WINDOW, 4 * WINDOW), 0)
        i = lax.rem(lax.broadcasted_iota(jnp.int32, (WINDOW, 4 * WINDOW), 1), WINDOW)
        before = jnp.where((j >= i) & (first > 0), scores[:WINDOW], masked_score)
        here = scores[WINDOW : 2 * WINDOW]
        after = jnp.where((j <= i) & (first + WINDOW < seq_len), scores[2 * WINDOW :], masked_score)
        top = jnp.max(jnp.maximum(jnp.maximum(before, here), after), axis=0, keepdims=True)
        top = jnp.maximum(top, sinks)
        before, here, after = jnp.exp(before - top), jnp.exp(here - top), jnp.exp(after - top)
        total = jnp.sum(before + here + after, axis=0, keepdims=True) + jnp.exp(sinks - top)
        inverse = 1.0 / total
        probs = jnp.concatenate([(r * inverse).astype(BF16) for r in (before, here, after)], axis=0)
        out = lax.dot_general(values, probs, TN, preferred_element_type=F32)
        out = jnp.concatenate([out[:, h * WINDOW : (h + 1) * WINDOW] for h in range(4)], axis=0)
        hid[n * WINDOW : (n + 1) * WINDOW, 0:256] = out.T.astype(BF16)

    def pool(n):
        first = offset + n * WINDOW
        i = lax.broadcasted_iota(jnp.int32, (WINDOW, WINDOW + 2 * RIM), 0)
        j = lax.broadcasted_iota(jnp.int32, (WINDOW, WINDOW + 2 * RIM), 1) - RIM
        pos = first + j
        member = (j >= i - half) & (j < i + half) & (pos >= 0) & (pos < seq_len)
        member = jnp.where(member, 1.0, 0.0).astype(BF16)
        sums = jnp.dot(member, chan[pl.ds(n * WINDOW, WINDOW + 2 * RIM), :], preferred_element_type=F32)
        t = first + lax.broadcasted_iota(jnp.int32, (WINDOW, 1), 0)
        count = (jnp.minimum(t + half, seq_len) - jnp.maximum(t - half, 0)).astype(F32)
        spread = (sums / count - chan[pl.ds(n * WINDOW + RIM, WINDOW), :].astype(F32)).astype(BF16)
        pooled = jnp.dot(spread, wpool[0], preferred_element_type=F32) * scale[...]
        hid[n * WINDOW : (n + 1) * WINDOW, 256:512] = pooled.astype(BF16)

    def mixers(first, second):
        for n in (first, second):
            pool(n)
            attend(n)

    def partials(first, second):
        both = jnp.concatenate([hid[chunk(first), :], hid[chunk(second), :]], axis=0)
        for d in (2, 1, 3, 0):
            cols = pl.ds(pl.multiple_of(lax.rem(y + d, NY) * feats, feats), feats)
            terms = lax.dot_general(both, wout_abs[cols, :], NT, preferred_element_type=F32).astype(BF16)
            part[d, chunk(first), :] = terms[:WINDOW]
            part[d, chunk(second), :] = terms[WINDOW:]

    via, straight, joined = {}, {}, {}
    for n in range(4):
        at = chunk(n)
        if n < 2:
            via[n] = message(part.at[2, at], relayed.at[at], dev_y(1))
            straight[n] = message(part.at[3, at], from_next.at[at], dev_y(-1))
            joined[n] = message(comb.at[at], from_prev.at[at], dev_y(1))
        else:
            via[n] = message(part.at[2, at], relayed.at[at], dev_y(-1))
            straight[n] = message(part.at[1, at], from_prev.at[at], dev_y(1))
            joined[n] = message(comb.at[at], from_next.at[at], dev_y(-1))

    def send(first, second):
        for copy in (via[first], via[second], straight[first], straight[second]):
            copy.start()

    def relay(n):
        at = chunk(n)
        via[n].wait_recv()
        mine = part[1 if n < 2 else 3, at, :]
        comb[at, :] = (mine.astype(F32) + relayed[at, :].astype(F32)).astype(BF16)
        joined[n].start()

    with jax.named_scope("mix12"):
        mixers(1, 2)
    with jax.named_scope("out_x_relay_far"):
        outof.relay_x(FAR_A)
        outof.relay_x(FAR_B)
    with jax.named_scope("halo"):
        for copy in halos:
            copy.wait_recv()
    with jax.named_scope("mix03"):
        mixers(0, 3)
    with jax.named_scope("out_last"):
        for b in (NEAR_A, NEAR_B):
            outof.last_x(b)
        for b in (OWN, NEAR_A, NEAR_B):
            outof.in_order(wout_abs, b)
        for b in (FAR_A, FAR_B):
            outof.last_x(b)
        for b in (FAR_A, FAR_B):
            outof.in_order(wout_abs, b)
    with jax.named_scope("part12"):
        partials(1, 2)
        send(1, 2)
    with jax.named_scope("part03"):
        partials(0, 3)
        send(0, 3)
    with jax.named_scope("relay12"):
        relay(1)
        relay(2)
    with jax.named_scope("relay03"):
        relay(0)
        relay(3)

    lane = lax.broadcasted_iota(jnp.int32, (WINDOW, 128), 1)
    told = []

    def settle(p, first, second):
        for k, n in enumerate((first, second)):
            at = chunk(n)
            straight[n].wait_recv()
            joined[n].wait_recv()
            mix = part[0, at, :].astype(F32) + from_prev[at, :].astype(F32) + from_next[at, :].astype(F32)
            share[at, :] = mix
            one = jnp.sum(mix, axis=1, keepdims=True)
            two = jnp.sum(mix * mix, axis=1, keepdims=True)
            both = jnp.where(lane == 0, one, jnp.where(lane == 1, two, 0.0))
            stats[0, p, k * 8 : k * 8 + 8, :] = both.T[0:8]
        told.append([
            message(stats.at[0, p], stats.at[2, p], dev_y(2)),
            message(stats.at[0, p], stats.at[3, p], dev_y(1)),
            message(stats.at[0, p], stats.at[1, p], dev_y(-1)),
        ])
        for copy in told[p]:
            copy.start()

    width = feats * NY
    writes = []

    def finish(p, first, second):
        for copy in told[p]:
            copy.wait_recv()
        for k, n in enumerate((first, second)):
            at = chunk(n)
            eight = slice(k * 8, k * 8 + 8)
            both = stats[0, p, eight, :] + stats[1, p, eight, :] + stats[2, p, eight, :] + stats[3, p, eight, :]
            both = jnp.concatenate([both] * 16, axis=0).T
            mean = both[:, 0:1] / width
            variance = both[:, 1:2] / width - mean * mean
            normed = (share[at, :] - mean) * lax.rsqrt(variance + epsilon) * gain[...]
            outv[at, :] = normed.astype(BF16)
            writes.append(pltpu.make_async_copy(outv.at[at], out_hbm.at[at], out_sem.at[n]))
            writes[-1].start()

    with jax.named_scope("settle12"):
        settle(0, 1, 2)
    with jax.named_scope("settle03"):
        settle(1, 0, 3)
    with jax.named_scope("finish12"):
        finish(0, 1, 2)
        for copy in used:
            copy.wait_send()
    with jax.named_scope("finish03"):
        finish(1, 0, 3)
        for write in writes:
            write.wait()


MESSAGES = 2 * (15 + 15 + 20) + 12 + 4 + 12 + 6


def local(tokens, w_query, w_key, w_value, w_pool_in, sink, w_pool, pool_scale, w_out_attn, w_out_pool, out_gain):
    rows, feats = tokens.shape
    hbm = pl.BlockSpec(memory_space=pltpu.HBM)
    lanes_in = 640
    lanes_out = 512
    model = feats * NY
    return pl.pallas_call(
        kernel,
        out_shape=jax.ShapeDtypeStruct((rows, feats), BF16),
        in_specs=[hbm] * 11,
        out_specs=hbm,
        scratch_shapes=[
            pltpu.VMEM((NY, rows, feats), BF16),
            pltpu.VMEM((NX, NC, NZ, 16, lanes_in), BF16),
            pltpu.VMEM((NX, NC, NZ, 16, lanes_out), BF16),
            pltpu.VMEM((model, lanes_in), BF16),
            pltpu.VMEM((model, lanes_out), BF16),
            pltpu.VMEM((rows, 256), BF16),
            pltpu.VMEM((rows + 2 * WINDOW, 128), BF16),
            pltpu.VMEM((rows + 2 * RIM, 256), BF16),
            pltpu.VMEM((rows, lanes_out), BF16),
            pltpu.VMEM((NY, rows, feats), BF16),
            pltpu.VMEM((rows, feats), BF16),
            pltpu.VMEM((rows, feats), BF16),
            pltpu.VMEM((rows, feats), BF16),
            pltpu.VMEM((rows, feats), BF16),
            pltpu.VMEM((rows, feats), F32),
            pltpu.VMEM((NY, 2, 16, 128), F32),
            pltpu.VMEM((16, 64), BF16),
            pltpu.VMEM((16, 64), BF16),
            pltpu.VMEM((1, 4), F32),
            pltpu.VMEM((1, 256, 256), BF16),
            pltpu.VMEM((1, 256), F32),
            pltpu.VMEM((1, 512), F32),
            pltpu.VMEM((rows, feats), BF16),
            pltpu.SemaphoreType.DMA((11,)),
            pltpu.SemaphoreType.DMA((4,)),
            pltpu.SemaphoreType.DMA((MESSAGES,)),
            pltpu.SemaphoreType.DMA((MESSAGES,)),
        ],
        compiler_params=pltpu.CompilerParams(
            collective_id=0, has_side_effects=True
        ),
    )(
        tokens, w_query, w_key, w_value, w_pool_in, sink.reshape(1, -1), w_pool, pool_scale.reshape(1, -1),
        w_out_attn.T, w_out_pool.T, out_gain.reshape(1, -1),
    )


def solution(mesh):
    finer = Mesh(mesh.devices.reshape(NZ, NX, NC, NY), (*SP, "tp"))
    return jax.shard_map(
        local,
        mesh=finer,
        in_specs=(
            P(SP, "tp"), P(SP, "tp"), P(SP, "tp"), P(SP, "tp"), P(SP, "tp"), P("tp"),
            P("tp", None, None), P("tp"), P("tp", SP), P("tp", SP), P("tp"),
        ),
        out_specs=P(SP, "tp"),
        check_vma=False,
    )
```

time: 85.3 us -> 80.2 us (0.940)
  the two profiles are of different devices: /device:TPU:32 before, /device:TPU:1 now
where the time goes in v2:
time: 80.2 us; the launch traced here: 80 us
  Pallas kernels  78.1 us (97%)
  local copies, waits for them, and re-layouts  1.87 us (2%)
    pallas_call x1, Pallas kernels, local(): pl.pallas_call(kernel, out_shape=jax.ShapeDtypeStruct((rows, feats), BF16...  78.1 us
    unnamed x1, local copies, waits for them, and re-layouts  1.87 us

profile of v2, /device:TPU:1, one launch (start us, length us, event | category | flops | bytes accessed | tf_op | source)
XLA Modules:
  0.0 80.0 jit_solution(14910353041989020715)
XLA Ops:
  0.0 78.1 %shard_map.109 = bf16[512,512]{1,0:T(8,128)(2,1)} custom-call(bf16[512,512]{1,0:T(8,128)(2,1)} %tok_hbm.1, bf16[16,256]{1,0:T(8,128)(2,1)} %wq_hbm.1, bf16[16,64]{1,0:T(8,128)(2,1)} %wk_hbm.1, bf16[16,64]{1,0:T(8,128)(2,1)} %wv_hbm.1, bf16[16,256]{1,0:T(8,128)(2,1)} %wc_hbm.1, f32[1,4]{1,0:T(1,128)} %bitcast.9, bf16[1,256,256]{2,1,0:T(8,128)(2,1)} %wpool_hbm.1, ...), custom_call_target="tpu_custom_call" | custom-call | tf_op jit(solution)/shard_map/pallas_call | solution.py:446
  78.1 1.9 %copy.13 = bf16[512,512]{1,0:T(8,128)(2,1)} copy(bf16[512,512]{1,0:T(8,128)(2,1)} %shard_map.109) | data formatting | bytes 1048576

commit v3 on v2

v3 whole, which is shorter than its diff:
```python
import jax
import jax.numpy as jnp
from jax import lax
from jax.experimental import pallas as pl
from jax.experimental.pallas import tpu as pltpu
from jax.sharding import Mesh
from jax.sharding import PartitionSpec as P

HEAD_DIM = 64
WINDOW = 128
RIM = 16
SP = ("sp_0", "sp_1", "sp_2")
MESH = pl.DeviceIdType.MESH
NZ, NX, NC, NY = 16, 4, 2, 4

epsilon = 1e-05
masked_score = -1e30

OWN, NEAR, FAR = 4, (0, 9), (9, 16)
FIRST, LOW, HIGH = (2, 7), (0, 2), (7, 9)
NT = (((1,), (1,)), ((), ()))
TN = (((0,), (0,)), ((), ()))
BF16, F32 = jnp.bfloat16, jnp.float32


def kernel(
    tok_hbm, wq_hbm, wk_hbm, wv_hbm, wc_hbm, sink_hbm, wpool_hbm, scale_hbm, woa_hbm, wop_hbm, gain_hbm,
    out_hbm,
    toks, win, wout, win_abs, wout_abs, query, kv, chan, hid, part, comb, relayed, from_prev, from_next,
    share, stats, wk, wv, sink, wpool, scale, gain, outv, local_sem, out_sem, sems,
):
    z, x, c, y = (lax.axis_index(a) for a in (*SP, "tp"))
    rows, feats = toks.shape[1], toks.shape[2]
    seq_len = rows * NZ * NX * NC
    place = (z * NX + x) * NC + c
    offset = place * rows
    total_places = NZ * NX * NC

    def dev_z(d):
        return {"sp_0": lax.rem(z + (d + NZ), NZ)}

    def dev_x(d):
        return {"sp_1": lax.rem(x + (d + NX), NX)}

    def dev_y(d):
        return {"tp": lax.rem(y + (d + NY), NY)}

    dev_c = {"sp_2": 1 - c}

    def dev_sp(d):
        s = lax.rem(place + (d + total_places), total_places)
        return {
            "sp_0": lax.div(s, NX * NC),
            "sp_1": lax.rem(lax.div(s, NC), NX),
            "sp_2": lax.rem(s, NC),
        }

    peers = [dev_z(d) for d in (4, -4, 3, -3, 2, -2, 1, -1)]
    peers += [dev_y(2), dev_x(2), dev_sp(1), dev_sp(-1), dev_x(1), dev_x(-1), dev_y(1), dev_y(-1), dev_c]
    barrier = pltpu.get_barrier_semaphore()
    for peer in peers:
        pl.semaphore_signal(barrier, inc=1, device_id=peer, device_id_type=MESH)

    mine_in, mine_out = win.at[OWN], wout.at[OWN]
    pairs = (
        (wk_hbm, wk), (wv_hbm, wv), (wq_hbm, mine_in.at[:, pl.ds(0, 256)]), (wc_hbm, mine_in.at[:, pl.ds(384, 256)]),
        (tok_hbm, toks.at[0]), (woa_hbm, mine_out.at[:, pl.ds(0, 256)]), (wop_hbm, mine_out.at[:, pl.ds(256, 256)]),
        (wpool_hbm, wpool), (scale_hbm, scale), (gain_hbm, gain), (sink_hbm, sink),
    )
    loads = [pltpu.make_async_copy(a, b, local_sem.at[k]) for k, (a, b) in enumerate(pairs)]
    for load in loads:
        load.start()

    with jax.named_scope("entry"):
        loads[0].wait()
        loads[1].wait()
        win[OWN, :, 256:384] = jnp.concatenate([wk[...], wv[...]], axis=1)
        for load in loads[2:]:
            load.wait()
        pl.semaphore_wait(barrier, len(peers))

    groups = {}

    def message(src, dst, device, sent, got):
        for key in (("send", sent), ("recv", got)):
            groups.setdefault(key, len(groups))
        return pltpu.make_async_remote_copy(
            src_ref=src, dst_ref=dst, send_sem=sems.at[groups["send", sent]], recv_sem=sems.at[groups["recv", got]],
            device_id=device, device_id_type=MESH,
        )

    def waiting(ref, kind, name):
        sem = sems.at[groups[kind, name]]
        copy = pltpu.make_async_remote_copy(
            src_ref=ref, dst_ref=ref, send_sem=sem, recv_sem=sem, device_id=dev_c, device_id_type=MESH
        )
        if kind == "send":
            copy.wait_send()
        else:
            copy.wait_recv()

    class Gather:
        def __init__(self, w, name):
            self.w, self.name = w, name

        def at(self, r, k, lo, hi):
            return self.w.at[pl.ds((r * NC + k) * NZ + lo, hi - lo)]

        def send(self, src, dst, device, got):
            message(src, dst, device, self.name, self.name + got).start()

        def wait(self, slots, got):
            waiting(self.w.at[pl.ds(0, slots)], "recv", self.name + got)

        def near(self):
            for d in (4, -4, 2, -2, 1, -1, 3, -3):
                p = (4 - d) % NZ
                got = {4: "m4", -4: "p4", 3: "n3", -3: "n3"}.get(d, "n1")
                self.send(self.at(0, 0, OWN, OWN + 1), self.at(0, 0, p, p + 1), dev_z(d), got)

        def far(self):
            self.wait(1, "m4")
            for e in (4, 3, 2, 1):
                self.send(self.at(0, 0, 0, 1), self.at(0, 0, 16 - e, 17 - e), dev_z(e), "far")
            self.wait(1, "p4")
            for e in (3, 2, 1):
                self.send(self.at(0, 0, 8, 9), self.at(0, 0, 8 + e, 9 + e), dev_z(-e), "far")

        def along_x(self, span):
            self.send(self.at(0, 0, *span), self.at(3, 0, *span), dev_x(1), "xp%d" % span[0])
            self.send(self.at(0, 0, *span), self.at(1, 0, *span), dev_x(-1), "xm%d" % span[0])

        def wait_x(self, r, span):
            self.wait(span[1] - span[0], ("xp%d" if r == 3 else "xm%d") % span[0])

        def relay_x(self, r, span):
            part = "near" if span[0] < 9 else "rest"
            self.send(self.at(r, 0, *span), self.at(2, 0, *span), dev_x(1 if r == 3 else -1), "x2" + part)

        def across(self, r, span):
            part = "near" if span[0] < 9 else "rest"
            self.send(self.at(r, 0, *span), self.at(r, 1, *span), dev_c, "c" + part)

        def first(self):
            self.wait(4, "n1")
            self.along_x(FIRST)

        def second(self):
            self.wait(2, "n3")
            self.along_x(LOW)
            self.along_x(HIGH)
            self.across(0, NEAR)

        def third(self):
            self.wait(7, "far")
            self.along_x(FAR)
            self.across(0, FAR)

        def relay_first(self):
            self.wait_x(3, FIRST)
            self.relay_x(3, (2, 5))
            self.wait_x(1, FIRST)
            self.relay_x(1, (5, 7))

        def relay_second(self):
            self.wait_x(3, LOW)
            self.relay_x(3, LOW)
            self.wait_x(1, HIGH)
            self.relay_x(1, HIGH)
            self.wait_x(3, HIGH)
            self.across(3, NEAR)
            self.wait_x(1, LOW)
            self.across(1, NEAR)

        def relay_third(self):
            self.wait_x(3, FAR)
            self.relay_x(3, (9, 12))
            self.across(3, FAR)
            self.wait_x(1, FAR)
            self.relay_x(1, (12, 16))
            self.across(1, FAR)

        def last_near(self):
            self.wait(9, "x2near")
            self.across(2, NEAR)

        def last_far(self):
            self.wait(7, "x2rest")
            self.across(2, FAR)

        def in_order(self, dest, span):
            w = self.w
            self.wait(NX * (span[1] - span[0]), "cnear" if span[0] < 9 else "crest")

            def one(p, carry):
                base = lax.rem(z + p + (NZ - 4), NZ) * (NX * NC * 16)
                for r in range(NX):
                    for k in range(NC):
                        at = base + lax.rem(x + r, NX) * (NC * 16) + lax.rem(c + k, NC) * 16
                        dest[pl.ds(pl.multiple_of(at, 16), 16), :] = w[(r * NC + k) * NZ + p]
                return carry

            lax.fori_loop(*span, one, 0)

        def sent(self):
            waiting(self.w.at[pl.ds(0, 127)], "send", self.name)

    into = Gather(win, "in")
    outof = Gather(wout, "out")

    def chunk(b):
        return pl.ds(b * WINDOW, WINDOW)

    def tokens_to(slot, b, src, d, got):
        message(toks.at[src, chunk(b)], toks.at[slot, chunk(b)], dev_y(d), "tok", got).start()

    def tokens_relay(b):
        waiting(toks.at[0, chunk(0)], "recv", "tok%d" % b)
        if b < 2:
            tokens_to(2, b, 3, 1, "tok")
        else:
            tokens_to(2, b, 1, -1, "tok")

    with jax.named_scope("near"):
        into.near()
        for b in (0, 1):
            tokens_to(3, b, 0, 1, "tok%d" % b)
            tokens_to(1, b + 2, 0, -1, "tok%d" % (b + 2))
        for b in (0, 1):
            tokens_to(3, b + 2, 0, 1, "tok")
            tokens_to(1, b, 0, -1, "tok")
    with jax.named_scope("in_first"):
        into.first()
    with jax.named_scope("in_far"):
        into.far()
        outof.near()
    with jax.named_scope("in_second"):
        into.second()
    with jax.named_scope("tok_relay_a"):
        tokens_relay(0)
        tokens_relay(2)
    with jax.named_scope("in_relay_first"):
        into.relay_first()
    with jax.named_scope("tok_relay_b"):
        tokens_relay(1)
        tokens_relay(3)
    with jax.named_scope("in_relay_second"):
        into.relay_second()
    with jax.named_scope("in_third"):
        into.third()
    with jax.named_scope("out_far"):
        outof.far()
    with jax.named_scope("in_last_near"):
        into.last_near()
    with jax.named_scope("in_relay_third"):
        into.relay_third()
    with jax.named_scope("out_first"):
        outof.first()
        outof.second()
    with jax.named_scope("in_order_near"):
        into.in_order(win_abs, NEAR)
    with jax.named_scope("out_third"):
        outof.third()
    with jax.named_scope("in_last_far"):
        into.last_far()
    with jax.named_scope("in_order_far"):
        into.in_order(win_abs, FAR)
    with jax.named_scope("tok_done"):
        waiting(toks.at[pl.ds(0, 2)], "recv", "tok")

    with jax.named_scope("project"):
        for lo, hi in ((256, 384), (384, 640), (0, 256)):
            acc = jnp.zeros((rows, hi - lo), F32)
            for r in range(NY):
                depth = pl.ds(pl.multiple_of(lax.rem(y + r, NY) * feats, feats), feats)
                acc = acc + jnp.dot(toks[r], win_abs[depth, lo:hi], preferred_element_type=F32)
            if lo == 256:
                kv[pl.ds(WINDOW, rows), :] = acc.astype(BF16)
            elif lo == 384:
                chan[pl.ds(RIM, rows), :] = acc.astype(BF16)
            else:
                query[...] = (acc * HEAD_DIM ** (-0.5)).astype(BF16)

    own_kv, own_ch = (kv, WINDOW, "kv"), (chan, RIM, "ch")
    for ref, size, name in (own_kv, own_ch):
        message(ref.at[pl.ds(rows, size)], ref.at[pl.ds(0, size)], dev_sp(1), name, name).start()
        message(ref.at[pl.ds(size, size)], ref.at[pl.ds(size + rows, size)], dev_sp(-1), name, name).start()

    with jax.named_scope("out_relay_first"):
        outof.relay_first()
        outof.relay_second()

    half = lax.shift_left(jnp.int32(1), y.astype(jnp.int32))
    sinks = jnp.concatenate([jnp.broadcast_to(sink[0:1, h : h + 1], (1, WINDOW)) for h in range(4)], axis=1)

    def attend(n):
        first = offset + n * WINDOW
        band = kv[pl.ds(n * WINDOW, 3 * WINDOW), :]
        keys, values = band[:, :HEAD_DIM], band[:, HEAD_DIM:]
        block = query[n * WINDOW : (n + 1) * WINDOW, :]
        stacked = jnp.concatenate([block[:, h * HEAD_DIM : (h + 1) * HEAD_DIM] for h in range(4)], axis=0)
        scores = lax.dot_general(keys, stacked, NT, preferred_element_type=F32)
        j = lax.broadcasted_iota(jnp.int32, (WINDOW, 4 * WINDOW), 0)
        i = lax.rem(lax.broadcasted_iota(jnp.int32, (WINDOW, 4 * WINDOW), 1), WINDOW)
        before = jnp.where((j >= i) & (first > 0), scores[:WINDOW], masked_score)
        here = scores[WINDOW : 2 * WINDOW]
        after = jnp.where((j <= i) & (first + WINDOW < seq_len), scores[2 * WINDOW :], masked_score)
        top = jnp.max(jnp.maximum(jnp.maximum(before, here), after), axis=0, keepdims=True)
        top = jnp.maximum(top, sinks)
        before, here, after = jnp.exp(before - top), jnp.exp(here - top), jnp.exp(after - top)
        total = jnp.sum(before + here + after, axis=0, keepdims=True) + jnp.exp(sinks - top)
        inverse = 1.0 / total
        probs = jnp.concatenate([(r * inverse).astype(BF16) for r in (before, here, after)], axis=0)
        out = lax.dot_general(values, probs, TN, preferred_element_type=F32)
        out = jnp.concatenate([out[:, h * WINDOW : (h + 1) * WINDOW] for h in range(4)], axis=0)
        hid[n * WINDOW : (n + 1) * WINDOW, 0:256] = out.T.astype(BF16)

    def pool(n):
        first = offset + n * WINDOW
        i = lax.broadcasted_iota(jnp.int32, (WINDOW, WINDOW + 2 * RIM), 0)
        j = lax.broadcasted_iota(jnp.int32, (WINDOW, WINDOW + 2 * RIM), 1) - RIM
        pos = first + j
        member = (j >= i - half) & (j < i + half) & (pos >= 0) & (pos < seq_len)
        member = jnp.where(member, 1.0, 0.0).astype(BF16)
        sums = jnp.dot(member, chan[pl.ds(n * WINDOW, WINDOW + 2 * RIM), :], preferred_element_type=F32)
        t = first + lax.broadcasted_iota(jnp.int32, (WINDOW, 1), 0)
        count = (jnp.minimum(t + half, seq_len) - jnp.maximum(t - half, 0)).astype(F32)
        spread = (sums / count - chan[pl.ds(n * WINDOW + RIM, WINDOW), :].astype(F32)).astype(BF16)
        pooled = jnp.dot(spread, wpool[0], preferred_element_type=F32) * scale[...]
        hid[n * WINDOW : (n + 1) * WINDOW, 256:512] = pooled.astype(BF16)

    def mixers(first, second):
        for n in (first, second):
            pool(n)
            attend(n)

    def partials(first, second):
        both = jnp.concatenate([hid[chunk(first), :], hid[chunk(second), :]], axis=0)
        for d in (2, 1, 3, 0):
            cols = pl.ds(pl.multiple_of(lax.rem(y + d, NY) * feats, feats), feats)
            terms = lax.dot_general(both, wout_abs[cols, :], NT, preferred_element_type=F32).astype(BF16)
            part[d, chunk(first), :] = terms[:WINDOW]
            part[d, chunk(second), :] = terms[WINDOW:]

    def send(first, second):
        for n in (first, second):
            message(part.at[2, chunk(n)], relayed.at[chunk(n)], dev_y(1 if n < 2 else -1), "sum", "via%d" % n).start()
        for n in (first, second):
            got = "sum%d" % (n in (0, 3))
            if n < 2:
                message(part.at[3, chunk(n)], from_next.at[chunk(n)], dev_y(-1), "sum", got).start()
            else:
                message(part.at[1, chunk(n)], from_prev.at[chunk(n)], dev_y(1), "sum", got).start()

    def relay(n):
        at = chunk(n)
        waiting(relayed.at[at], "recv", "via%d" % n)
        mine = part[1 if n < 2 else 3, at, :]
        comb[at, :] = (mine.astype(F32) + relayed[at, :].astype(F32)).astype(BF16)
        got = "sum%d" % (n in (0, 3))
        if n < 2:
            message(comb.at[at], from_prev.at[at], dev_y(1), "sum", got).start()
        else:
            message(comb.at[at], from_next.at[at], dev_y(-1), "sum", got).start()

    with jax.named_scope("mix12"):
        mixers(1, 2)
    with jax.named_scope("out_relay_third"):
        outof.last_near()
        outof.relay_third()
    with jax.named_scope("halo"):
        waiting(kv.at[pl.ds(0, 2 * WINDOW)], "recv", "kv")
        waiting(chan.at[pl.ds(0, 2 * RIM)], "recv", "ch")
    with jax.named_scope("mix03"):
        mixers(0, 3)
    with jax.named_scope("out_last"):
        outof.in_order(wout_abs, NEAR)
        outof.last_far()
        outof.in_order(wout_abs, FAR)
    with jax.named_scope("part12"):
        partials(1, 2)
        send(1, 2)
    with jax.named_scope("part03"):
        partials(0, 3)
        send(0, 3)
    with jax.named_scope("relay12"):
        relay(1)
        relay(2)
    with jax.named_scope("relay03"):
        relay(0)
        relay(3)

    lane = lax.broadcasted_iota(jnp.int32, (WINDOW, 128), 1)

    def settle(p, first, second):
        waiting(from_prev, "recv", "sum%d" % p)
        for k, n in enumerate((first, second)):
            at = chunk(n)
            mix = part[0, at, :].astype(F32) + from_prev[at, :].astype(F32) + from_next[at, :].astype(F32)
            share[at, :] = mix
            one = jnp.sum(mix, axis=1, keepdims=True)
            two = jnp.sum(mix * mix, axis=1, keepdims=True)
            both = jnp.where(lane == 0, one, jnp.where(lane == 1, two, 0.0))
            stats[4 * p, k * 8 : k * 8 + 8, :] = both.T[0:8]
        for d, slot in ((2, 2), (1, 3), (-1, 1)):
            message(stats.at[4 * p], stats.at[4 * p + slot], dev_y(d), "told%d" % p, "told%d" % p).start()

    width = feats * NY
    writes = []

    def finish(p, first, second):
        waiting(stats.at[pl.ds(0, 3)], "recv", "told%d" % p)
        for k, n in enumerate((first, second)):
            at = chunk(n)
            eight = slice(k * 8, k * 8 + 8)
            both = stats[4 * p, eight, :] + stats[4 * p + 1, eight, :]
            both = both + stats[4 * p + 2, eight, :] + stats[4 * p + 3, eight, :]
            both = jnp.concatenate([both] * 16, axis=0).T
            mean = both[:, 0:1] / width
            variance = both[:, 1:2] / width - mean * mean
            normed = (share[at, :] - mean) * lax.rsqrt(variance + epsilon) * gain[...]
            outv[at, :] = normed.astype(BF16)
            writes.append(pltpu.make_async_copy(outv.at[at], out_hbm.at[at], out_sem.at[n]))
            writes[-1].start()

    with jax.named_scope("settle12"):
        settle(0, 1, 2)
    with jax.named_scope("settle03"):
        settle(1, 0, 3)
    with jax.named_scope("finish12"):
        finish(0, 1, 2)
        into.sent()
        outof.sent()
        for ref, name in (
            (toks.at[pl.ds(0, 3)], "tok"), (part.at[pl.ds(0, 3)], "sum"), (kv.at[pl.ds(0, 2 * WINDOW)], "kv"),
            (chan.at[pl.ds(0, 2 * RIM)], "ch"), (stats.at[pl.ds(0, 3)], "told0"), (stats.at[pl.ds(0, 3)], "told1"),
        ):
            waiting(ref, "send", name)
    with jax.named_scope("finish03"):
        finish(1, 0, 3)
        for write in writes:
            write.wait()
    assert len(groups) == SEMAPHORES


SEMAPHORES = 57


def local(tokens, w_query, w_key, w_value, w_pool_in, sink, w_pool, pool_scale, w_out_attn, w_out_pool, out_gain):
    rows, feats = tokens.shape
    hbm = pl.BlockSpec(memory_space=pltpu.HBM)
    lanes_in = 640
    lanes_out = 512
    model = feats * NY
    return pl.pallas_call(
        kernel,
        out_shape=jax.ShapeDtypeStruct((rows, feats), BF16),
        in_specs=[hbm] * 11,
        out_specs=hbm,
        scratch_shapes=[
            pltpu.VMEM((NY, rows, feats), BF16),
            pltpu.VMEM((NX * NC * NZ, 16, lanes_in), BF16),
            pltpu.VMEM((NX * NC * NZ, 16, lanes_out), BF16),
            pltpu.VMEM((model, lanes_in), BF16),
            pltpu.VMEM((model, lanes_out), BF16),
            pltpu.VMEM((rows, 256), BF16),
            pltpu.VMEM((rows + 2 * WINDOW, 128), BF16),
            pltpu.VMEM((rows + 2 * RIM, 256), BF16),
            pltpu.VMEM((rows, lanes_out), BF16),
            pltpu.VMEM((NY, rows, feats), BF16),
            pltpu.VMEM((rows, feats), BF16),
            pltpu.VMEM((rows, feats), BF16),
            pltpu.VMEM((rows, feats), BF16),
            pltpu.VMEM((rows, feats), BF16),
            pltpu.VMEM((rows, feats), F32),
            pltpu.VMEM((2 * NY, 16, 128), F32),
            pltpu.VMEM((16, 64), BF16),
            pltpu.VMEM((16, 64), BF16),
            pltpu.VMEM((1, 4), F32),
            pltpu.VMEM((1, 256, 256), BF16),
            pltpu.VMEM((1, 256), F32),
            pltpu.VMEM((1, 512), F32),
            pltpu.VMEM((rows, feats), BF16),
            pltpu.SemaphoreType.DMA((11,)),
            pltpu.SemaphoreType.DMA((4,)),
            pltpu.SemaphoreType.DMA((SEMAPHORES,)),
        ],
        compiler_params=pltpu.CompilerParams(
            collective_id=0, has_side_effects=True
        ),
    )(
        tokens, w_query, w_key, w_value, w_pool_in, sink.reshape(1, -1), w_pool, pool_scale.reshape(1, -1),
        w_out_attn.T, w_out_pool.T, out_gain.reshape(1, -1),
    )


def solution(mesh):
    finer = Mesh(mesh.devices.reshape(NZ, NX, NC, NY), (*SP, "tp"))
    return jax.shard_map(
        local,
        mesh=finer,
        in_specs=(
            P(SP, "tp"), P(SP, "tp"), P(SP, "tp"), P(SP, "tp"), P(SP, "tp"), P("tp"),
            P("tp", None, None), P("tp"), P("tp", SP), P("tp", SP), P("tp"),
        ),
        out_specs=P(SP, "tp"),
        check_vma=False,
    )
```

time: 80.2 us -> 76.4 us (0.953)
  Pallas kernels: 78.1 us -> 74.3 us
    pallas_call x1, Pallas kernels: 78.1 us -> 74.3 us  [local(): pl.pallas_call(kernel, out_shape=jax.ShapeDtypeStruct((rows, feats), BF16...]
where the time goes in v3:
time: 76.4 us; the launch traced here: 76.2 us
  Pallas kernels  74.3 us (97%)
  local copies, waits for them, and re-layouts  1.87 us (2%)
    pallas_call x1, Pallas kernels, local(): pl.pallas_call(kernel, out_shape=jax.ShapeDtypeStruct((rows, feats), BF16...  74.3 us
    unnamed x1, local copies, waits for them, and re-layouts  1.87 us

profile of v3, /device:TPU:1, one launch (start us, length us, event | category | flops | bytes accessed | tf_op | source)
XLA Modules:
  0.0 76.2 jit_solution(1224960031374669826)
XLA Ops:
  0.0 74.3 %shard_map.109 = bf16[512,512]{1,0:T(8,128)(2,1)} custom-call(bf16[512,512]{1,0:T(8,128)(2,1)} %tok_hbm.1, bf16[16,256]{1,0:T(8,128)(2,1)} %wq_hbm.1, bf16[16,64]{1,0:T(8,128)(2,1)} %wk_hbm.1, bf16[16,64]{1,0:T(8,128)(2,1)} %wv_hbm.1, bf16[16,256]{1,0:T(8,128)(2,1)} %wc_hbm.1, f32[1,4]{1,0:T(1,128)} %bitcast.9, bf16[1,256,256]{2,1,0:T(8,128)(2,1)} %wpool_hbm.1, ...), custom_call_target="tpu_custom_call" | custom-call | tf_op jit(solution)/shard_map/pallas_call | solution.py:455
  74.3 1.9 %copy.13 = bf16[512,512]{1,0:T(8,128)(2,1)} copy(bf16[512,512]{1,0:T(8,128)(2,1)} %shard_map.109) | data formatting | bytes 1048576

commit v4 on v3

--- a/solution.py
+++ b/solution.py
@@ -113,7 +113,7 @@
             waiting(self.w.at[pl.ds(0, slots)], "recv", self.name + got)
 
         def near(self):
-            for d in (4, -4, 2, -2, 1, -1, 3, -3):
+            for d in (1, -1, 2, -2, 4, -4, 3, -3):
                 p = (4 - d) % NZ
                 got = {4: "m4", -4: "p4", 3: "n3", -3: "n3"}.get(d, "n1")
                 self.send(self.at(0, 0, OWN, OWN + 1), self.at(0, 0, p, p + 1), dev_z(d), got)
@@ -248,17 +248,21 @@
         into.relay_second()
     with jax.named_scope("in_third"):
         into.third()
+    with jax.named_scope("in_last_near"):
+        into.last_near()
+    with jax.named_scope("out_first"):
+        outof.first()
     with jax.named_scope("out_far"):
         outof.far()
-    with jax.named_scope("in_last_near"):
-        into.last_near()
+    with jax.named_scope("out_second"):
+        outof.second()
     with jax.named_scope("in_relay_third"):
         into.relay_third()
-    with jax.named_scope("out_first"):
-        outof.first()
-        outof.second()
     with jax.named_scope("in_order_near"):
         into.in_order(win_abs, NEAR)
+    with jax.named_scope("out_relay_first"):
+        outof.relay_first()
+        outof.relay_second()
     with jax.named_scope("out_third"):
         outof.third()
     with jax.named_scope("in_last_far"):
@@ -268,27 +272,28 @@
     with jax.named_scope("tok_done"):
         waiting(toks.at[pl.ds(0, 2)], "recv", "tok")
 
-    with jax.named_scope("project"):
-        for lo, hi in ((256, 384), (384, 640), (0, 256)):
-            acc = jnp.zeros((rows, hi - lo), F32)
-            for r in range(NY):
-                depth = pl.ds(pl.multiple_of(lax.rem(y + r, NY) * feats, feats), feats)
-                acc = acc + jnp.dot(toks[r], win_abs[depth, lo:hi], preferred_element_type=F32)
-            if lo == 256:
-                kv[pl.ds(WINDOW, rows), :] = acc.astype(BF16)
-            elif lo == 384:
-                chan[pl.ds(RIM, rows), :] = acc.astype(BF16)
-            else:
-                query[...] = (acc * HEAD_DIM ** (-0.5)).astype(BF16)
+    def project(lo, hi):
+        acc = jnp.zeros((rows, hi - lo), F32)
+        for r in range(NY):
+            depth = pl.ds(pl.multiple_of(lax.rem(y + r, NY) * feats, feats), feats)
+            acc = acc + jnp.dot(toks[r], win_abs[depth, lo:hi], preferred_element_type=F32)
+        return acc
 
     own_kv, own_ch = (kv, WINDOW, "kv"), (chan, RIM, "ch")
-    for ref, size, name in (own_kv, own_ch):
+
+    def to_neighbours(ref, size, name):
         message(ref.at[pl.ds(rows, size)], ref.at[pl.ds(0, size)], dev_sp(1), name, name).start()
         message(ref.at[pl.ds(size, size)], ref.at[pl.ds(size + rows, size)], dev_sp(-1), name, name).start()
 
-    with jax.named_scope("out_relay_first"):
-        outof.relay_first()
-        outof.relay_second()
+    with jax.named_scope("project"):
+        kv[pl.ds(WINDOW, rows), :] = project(256, 384).astype(BF16)
+        chan[pl.ds(RIM, rows), :] = project(384, 640).astype(BF16)
+        query[...] = (project(0, 256) * HEAD_DIM ** (-0.5)).astype(BF16)
+        to_neighbours(*own_kv)
+        to_neighbours(*own_ch)
+    with jax.named_scope("out_relay_third"):
+        outof.relay_third()
+        outof.last_near()
 
     half = lax.shift_left(jnp.int32(1), y.astype(jnp.int32))
     sinks = jnp.concatenate([jnp.broadcast_to(sink[0:1, h : h + 1], (1, WINDOW)) for h in range(4)], axis=1)
@@ -334,23 +339,21 @@
             pool(n)
             attend(n)
 
-    def partials(first, second):
+    def partials(p, first, second):
         both = jnp.concatenate([hid[chunk(first), :], hid[chunk(second), :]], axis=0)
-        for d in (2, 1, 3, 0):
+        for d in (2, 3, 1, 0):
             cols = pl.ds(pl.multiple_of(lax.rem(y + d, NY) * feats, feats), feats)
             terms = lax.dot_general(both, wout_abs[cols, :], NT, preferred_element_type=F32).astype(BF16)
             part[d, chunk(first), :] = terms[:WINDOW]
             part[d, chunk(second), :] = terms[WINDOW:]
-
-    def send(first, second):
         for n in (first, second):
-            message(part.at[2, chunk(n)], relayed.at[chunk(n)], dev_y(1 if n < 2 else -1), "sum", "via%d" % n).start()
+            target = dev_y(1 if n < 2 else -1)
+            message(part.at[2, chunk(n)], relayed.at[chunk(n)], target, "sum", "via%d" % n).start()
         for n in (first, second):
-            got = "sum%d" % (n in (0, 3))
             if n < 2:
-                message(part.at[3, chunk(n)], from_next.at[chunk(n)], dev_y(-1), "sum", got).start()
+                message(part.at[3, chunk(n)], from_next.at[chunk(n)], dev_y(-1), "sum", "sum%d" % p).start()
             else:
-                message(part.at[1, chunk(n)], from_prev.at[chunk(n)], dev_y(1), "sum", got).start()
+                message(part.at[1, chunk(n)], from_prev.at[chunk(n)], dev_y(1), "sum", "sum%d" % p).start()
 
     def relay(n):
         at = chunk(n)
@@ -365,24 +368,21 @@
 
     with jax.named_scope("mix12"):
         mixers(1, 2)
-    with jax.named_scope("out_relay_third"):
-        outof.last_near()
-        outof.relay_third()
+    with jax.named_scope("out_order_near"):
+        outof.in_order(wout_abs, NEAR)
+    with jax.named_scope("out_last_far"):
+        outof.last_far()
     with jax.named_scope("halo"):
         waiting(kv.at[pl.ds(0, 2 * WINDOW)], "recv", "kv")
         waiting(chan.at[pl.ds(0, 2 * RIM)], "recv", "ch")
     with jax.named_scope("mix03"):
         mixers(0, 3)
     with jax.named_scope("out_last"):
-        outof.in_order(wout_abs, NEAR)
-        outof.last_far()
         outof.in_order(wout_abs, FAR)
     with jax.named_scope("part12"):
-        partials(1, 2)
-        send(1, 2)
+        partials(0, 1, 2)
     with jax.named_scope("part03"):
-        partials(0, 3)
-        send(0, 3)
+        partials(1, 0, 3)
     with jax.named_scope("relay12"):
         relay(1)
         relay(2)

time: 76.4 us -> 73.1 us (0.957)
  Pallas kernels: 74.3 us -> 71.1 us
    pallas_call x1, Pallas kernels: 74.3 us -> 71.1 us  [local(): pl.pallas_call(kernel, out_shape=jax.ShapeDtypeStruct((rows, feats), BF16...]
where the time goes in v4:
time: 73.1 us; the launch traced here: 73 us
  Pallas kernels  71.1 us (97%)
  local copies, waits for them, and re-layouts  1.87 us (3%)
    pallas_call x1, Pallas kernels, local(): pl.pallas_call(kernel, out_shape=jax.ShapeDtypeStruct((rows, feats), BF16...  71.1 us
    unnamed x1, local copies, waits for them, and re-layouts  1.87 us

profile of v4, /device:TPU:1, one launch (start us, length us, event | category | flops | bytes accessed | tf_op | source)
XLA Modules:
  0.0 73.0 jit_solution(2875834271216372341)
XLA Ops:
  0.0 71.1 %shard_map.109 = bf16[512,512]{1,0:T(8,128)(2,1)} custom-call(bf16[512,512]{1,0:T(8,128)(2,1)} %tok_hbm.1, bf16[16,256]{1,0:T(8,128)(2,1)} %wq_hbm.1, bf16[16,64]{1,0:T(8,128)(2,1)} %wk_hbm.1, bf16[16,64]{1,0:T(8,128)(2,1)} %wv_hbm.1, bf16[16,256]{1,0:T(8,128)(2,1)} %wc_hbm.1, f32[1,4]{1,0:T(1,128)} %bitcast.9, bf16[1,256,256]{2,1,0:T(8,128)(2,1)} %wpool_hbm.1, ...), custom_call_target="tpu_custom_call" | custom-call | tf_op jit(solution)/shard_map/pallas_call | solution.py:455
  71.1 1.9 %copy.13 = bf16[512,512]{1,0:T(8,128)(2,1)} copy(bf16[512,512]{1,0:T(8,128)(2,1)} %shard_map.109) | data formatting | bytes 1048576

commit v5 on v4

--- a/solution.py
+++ b/solution.py
@@ -17,7 +17,7 @@
 masked_score = -1e30
 
 OWN, NEAR, FAR = 4, (0, 9), (9, 16)
-FIRST, LOW, HIGH = (2, 7), (0, 2), (7, 9)
+FIRST, SECOND, THIRD = ((2, 5), (5, 7)), ((0, 2), (7, 9)), ((9, 12), (12, 16))
 NT = (((1,), (1,)), ((), ()))
 TN = (((0,), (0,)), ((), ()))
 BF16, F32 = jnp.bfloat16, jnp.float32
@@ -27,7 +27,7 @@
     tok_hbm, wq_hbm, wk_hbm, wv_hbm, wc_hbm, sink_hbm, wpool_hbm, scale_hbm, woa_hbm, wop_hbm, gain_hbm,
     out_hbm,
     toks, win, wout, win_abs, wout_abs, query, kv, chan, hid, part, comb, relayed, from_prev, from_next,
-    share, stats, wk, wv, sink, wpool, scale, gain, outv, local_sem, out_sem, sems,
+    share, stats, turned_toks, acc, wk, wv, sink, wpool, scale, gain, outv, local_sem, out_sem, sems,
 ):
     z, x, c, y = (lax.axis_index(a) for a in (*SP, "tp"))
     rows, feats = toks.shape[1], toks.shape[2]
@@ -56,26 +56,26 @@
         }
 
     peers = [dev_z(d) for d in (4, -4, 3, -3, 2, -2, 1, -1)]
-    peers += [dev_y(2), dev_x(2), dev_sp(1), dev_sp(-1), dev_x(1), dev_x(-1), dev_y(1), dev_y(-1), dev_c]
-    barrier = pltpu.get_barrier_semaphore()
-    for peer in peers:
-        pl.semaphore_signal(barrier, inc=1, device_id=peer, device_id_type=MESH)
-
+    peers += [dev_y(2), dev_sp(1), dev_sp(-1), dev_x(1), dev_x(-1), dev_y(1), dev_y(-1), dev_c]
     mine_in, mine_out = win.at[OWN], wout.at[OWN]
     pairs = (
         (wk_hbm, wk), (wv_hbm, wv), (wq_hbm, mine_in.at[:, pl.ds(0, 256)]), (wc_hbm, mine_in.at[:, pl.ds(384, 256)]),
-        (tok_hbm, toks.at[0]), (woa_hbm, mine_out.at[:, pl.ds(0, 256)]), (wop_hbm, mine_out.at[:, pl.ds(256, 256)]),
+        (woa_hbm, mine_out.at[:, pl.ds(0, 256)]), (wop_hbm, mine_out.at[:, pl.ds(256, 256)]), (tok_hbm, toks.at[0]),
         (wpool_hbm, wpool), (scale_hbm, scale), (gain_hbm, gain), (sink_hbm, sink),
     )
     loads = [pltpu.make_async_copy(a, b, local_sem.at[k]) for k, (a, b) in enumerate(pairs)]
     for load in loads:
         load.start()
 
+    barrier = pltpu.get_barrier_semaphore()
+    for peer in peers:
+        pl.semaphore_signal(barrier, inc=1, device_id=peer, device_id_type=MESH)
+
     with jax.named_scope("entry"):
         loads[0].wait()
         loads[1].wait()
         win[OWN, :, 256:384] = jnp.concatenate([wk[...], wv[...]], axis=1)
-        for load in loads[2:]:
+        for load in loads[2:6]:
             load.wait()
         pl.semaphore_wait(barrier, len(peers))
 
@@ -126,16 +126,19 @@
             for e in (3, 2, 1):
                 self.send(self.at(0, 0, 8, 9), self.at(0, 0, 8 + e, 9 + e), dev_z(-e), "far")
 
-        def along_x(self, span):
-            self.send(self.at(0, 0, *span), self.at(3, 0, *span), dev_x(1), "xp%d" % span[0])
-            self.send(self.at(0, 0, *span), self.at(1, 0, *span), dev_x(-1), "xm%d" % span[0])
-
-        def wait_x(self, r, span):
-            self.wait(span[1] - span[0], ("xp%d" if r == 3 else "xm%d") % span[0])
-
-        def relay_x(self, r, span):
-            part = "near" if span[0] < 9 else "rest"
-            self.send(self.at(r, 0, *span), self.at(2, 0, *span), dev_x(1 if r == 3 else -1), "x2" + part)
+        def along_x(self, stage):
+            up, down = stage
+            others = "o%d" % (stage is THIRD)
+            self.send(self.at(0, 0, *up), self.at(3, 0, *up), dev_x(1), "x%d" % up[0])
+            self.send(self.at(0, 0, *down), self.at(1, 0, *down), dev_x(-1), "x%d" % down[0])
+            self.send(self.at(0, 0, *down), self.at(3, 0, *down), dev_x(1), others)
+            self.send(self.at(0, 0, *up), self.at(1, 0, *up), dev_x(-1), others)
+
+        def relay_x(self, stage):
+            part = "rest" if stage is THIRD else "near"
+            for r, d, span in ((3, 1, stage[0]), (1, -1, stage[1])):
+                self.wait(span[1] - span[0], "x%d" % span[0])
+                self.send(self.at(r, 0, *span), self.at(2, 0, *span), dev_x(d), "x2" + part)
 
         def across(self, r, span):
             part = "near" if span[0] < 9 else "rest"
@@ -147,37 +150,22 @@
 
         def second(self):
             self.wait(2, "n3")
-            self.along_x(LOW)
-            self.along_x(HIGH)
+            self.along_x(SECOND)
             self.across(0, NEAR)
 
         def third(self):
             self.wait(7, "far")
-            self.along_x(FAR)
+            self.along_x(THIRD)
             self.across(0, FAR)
 
-        def relay_first(self):
-            self.wait_x(3, FIRST)
-            self.relay_x(3, (2, 5))
-            self.wait_x(1, FIRST)
-            self.relay_x(1, (5, 7))
-
-        def relay_second(self):
-            self.wait_x(3, LOW)
-            self.relay_x(3, LOW)
-            self.wait_x(1, HIGH)
-            self.relay_x(1, HIGH)
-            self.wait_x(3, HIGH)
+        def others_near(self):
+            self.wait(9, "o0")
             self.across(3, NEAR)
-            self.wait_x(1, LOW)
             self.across(1, NEAR)
 
-        def relay_third(self):
-            self.wait_x(3, FAR)
-            self.relay_x(3, (9, 12))
+        def others_far(self):
+            self.wait(7, "o1")
             self.across(3, FAR)
-            self.wait_x(1, FAR)
-            self.relay_x(1, (12, 16))
             self.across(1, FAR)
 
         def last_near(self):
@@ -188,12 +176,12 @@
             self.wait(7, "x2rest")
             self.across(2, FAR)
 
-        def in_order(self, dest, span):
+        def in_order(self, dest, span, turned):
             w = self.w
             self.wait(NX * (span[1] - span[0]), "cnear" if span[0] < 9 else "crest")
 
             def one(p, carry):
-                base = lax.rem(z + p + (NZ - 4), NZ) * (NX * NC * 16)
+                base = (lax.rem(z + p + (NZ - 4), NZ) if turned else p) * (NX * NC * 16)
                 for r in range(NX):
                     for k in range(NC):
                         at = base + lax.rem(x + r, NX) * (NC * 16) + lax.rem(c + k, NC) * 16
@@ -223,6 +211,7 @@
 
     with jax.named_scope("near"):
         into.near()
+        loads[6].wait()
         for b in (0, 1):
             tokens_to(3, b, 0, 1, "tok%d" % b)
             tokens_to(1, b + 2, 0, -1, "tok%d" % (b + 2))
@@ -234,50 +223,69 @@
     with jax.named_scope("in_far"):
         into.far()
         outof.near()
+        for load in loads[7:]:
+            load.wait()
     with jax.named_scope("in_second"):
         into.second()
     with jax.named_scope("tok_relay_a"):
         tokens_relay(0)
         tokens_relay(2)
     with jax.named_scope("in_relay_first"):
-        into.relay_first()
+        into.relay_x(FIRST)
     with jax.named_scope("tok_relay_b"):
         tokens_relay(1)
         tokens_relay(3)
     with jax.named_scope("in_relay_second"):
-        into.relay_second()
+        into.relay_x(SECOND)
     with jax.named_scope("in_third"):
         into.third()
+    with jax.named_scope("in_others_near"):
+        into.others_near()
+    with jax.named_scope("out_far"):
+        outof.far()
+    with jax.named_scope("out_first"):
+        outof.first()
     with jax.named_scope("in_last_near"):
         into.last_near()
-    with jax.named_scope("out_first"):
-        outof.first()
-    with jax.named_scope("out_far"):
-        outof.far()
+    with jax.named_scope("in_relay_third"):
+        into.relay_x(THIRD)
     with jax.named_scope("out_second"):
         outof.second()
-    with jax.named_scope("in_relay_third"):
-        into.relay_third()
     with jax.named_scope("in_order_near"):
-        into.in_order(win_abs, NEAR)
+        into.in_order(win_abs, NEAR, False)
+    with jax.named_scope("in_others_far"):
+        into.others_far()
     with jax.named_scope("out_relay_first"):
-        outof.relay_first()
-        outof.relay_second()
+        outof.relay_x(FIRST)
     with jax.named_scope("out_third"):
         outof.third()
     with jax.named_scope("in_last_far"):
         into.last_far()
-    with jax.named_scope("in_order_far"):
-        into.in_order(win_abs, FAR)
     with jax.named_scope("tok_done"):
         waiting(toks.at[pl.ds(0, 2)], "recv", "tok")
+        for p in range(NZ):
+            at = lax.rem(z + (p + NZ - 4), NZ)
+            per = feats // 128
+            r = lax.rem(lax.div(at, per) + (NY - y), NY)
+            cols = pl.ds(pl.multiple_of(lax.rem(at, per) * 128, 128), 128)
+            turned_toks[:, p * 128 : (p + 1) * 128] = toks[r, :, cols]
+
+    parts = ((256, 384), (384, 640), (0, 256))
+    with jax.named_scope("project_near"):
+        depth = slice(NEAR[0] * 128, NEAR[1] * 128)
+        for lo, hi in parts:
+            acc[:, lo:hi] = jnp.dot(turned_toks[:, depth], win_abs[depth, lo:hi], preferred_element_type=F32)
+    with jax.named_scope("out_relay_second"):
+        outof.relay_x(SECOND)
+        outof.others_near()
+    with jax.named_scope("in_order_far"):
+        into.in_order(win_abs, FAR, False)
+    with jax.named_scope("out_relay_third"):
+        outof.relay_x(THIRD)
 
     def project(lo, hi):
-        acc = jnp.zeros((rows, hi - lo), F32)
-        for r in range(NY):
-            depth = pl.ds(pl.multiple_of(lax.rem(y + r, NY) * feats, feats), feats)
-            acc = acc + jnp.dot(toks[r], win_abs[depth, lo:hi], preferred_element_type=F32)
-        return acc
+        depth = slice(FAR[0] * 128, FAR[1] * 128)
+        return acc[:, lo:hi] + jnp.dot(turned_toks[:, depth], win_abs[depth, lo:hi], preferred_element_type=F32)
 
     own_kv, own_ch = (kv, WINDOW, "kv"), (chan, RIM, "ch")
 
@@ -291,9 +299,9 @@
         query[...] = (project(0, 256) * HEAD_DIM ** (-0.5)).astype(BF16)
         to_neighbours(*own_kv)
         to_neighbours(*own_ch)
-    with jax.named_scope("out_relay_third"):
-        outof.relay_third()
+    with jax.named_scope("out_last_near"):
         outof.last_near()
+        outof.others_far()
 
     half = lax.shift_left(jnp.int32(1), y.astype(jnp.int32))
     sinks = jnp.concatenate([jnp.broadcast_to(sink[0:1, h : h + 1], (1, WINDOW)) for h in range(4)], axis=1)
@@ -334,8 +342,8 @@
         pooled = jnp.dot(spread, wpool[0], preferred_element_type=F32) * scale[...]
         hid[n * WINDOW : (n + 1) * WINDOW, 256:512] = pooled.astype(BF16)
 
-    def mixers(first, second):
-        for n in (first, second):
+    def mixers(*which):
+        for n in which:
             pool(n)
             attend(n)
 
@@ -366,21 +374,23 @@
         else:
             message(comb.at[at], from_next.at[at], dev_y(-1), "sum", got).start()
 
-    with jax.named_scope("mix12"):
-        mixers(1, 2)
-    with jax.named_scope("out_order_near"):
-        outof.in_order(wout_abs, NEAR)
+    with jax.named_scope("mix1"):
+        mixers(1)
     with jax.named_scope("out_last_far"):
         outof.last_far()
+    with jax.named_scope("mix2"):
+        mixers(2)
+    with jax.named_scope("out_order_near"):
+        outof.in_order(wout_abs, NEAR, True)
+    with jax.named_scope("out_order_far"):
+        outof.in_order(wout_abs, FAR, True)
+    with jax.named_scope("part12"):
+        partials(0, 1, 2)
     with jax.named_scope("halo"):
         waiting(kv.at[pl.ds(0, 2 * WINDOW)], "recv", "kv")
         waiting(chan.at[pl.ds(0, 2 * RIM)], "recv", "ch")
     with jax.named_scope("mix03"):
         mixers(0, 3)
-    with jax.named_scope("out_last"):
-        outof.in_order(wout_abs, FAR)
-    with jax.named_scope("part12"):
-        partials(0, 1, 2)
     with jax.named_scope("part03"):
         partials(1, 0, 3)
     with jax.named_scope("relay12"):
@@ -474,6 +484,8 @@
             pltpu.VMEM((rows, feats), BF16),
             pltpu.VMEM((rows, feats), F32),
             pltpu.VMEM((2 * NY, 16, 128), F32),
+            pltpu.VMEM((rows, model), BF16),
+            pltpu.VMEM((rows, lanes_in), F32),
             pltpu.VMEM((16, 64), BF16),
             pltpu.VMEM((16, 64), BF16),
             pltpu.VMEM((1, 4), F32),

time: 73.1 us -> 71.7 us (0.981)
  Pallas kernels: 71.1 us -> 69.5 us
    pallas_call x1, Pallas kernels: 71.1 us -> 69.5 us  [local(): pl.pallas_call(kernel, out_shape=jax.ShapeDtypeStruct((rows, feats), BF16...]
where the time goes in v5:
time: 71.7 us; the launch traced here: 71.4 us
  Pallas kernels  69.5 us (97%)
  local copies, waits for them, and re-layouts  1.87 us (3%)
    pallas_call x1, Pallas kernels, local(): pl.pallas_call(kernel, out_shape=jax.ShapeDtypeStruct((rows, feats), BF16...  69.5 us
    unnamed x1, local copies, waits for them, and re-layouts  1.87 us

profile of v5, /device:TPU:1, one launch (start us, length us, event | category | flops | bytes accessed | tf_op | source)
XLA Modules:
  0.0 71.4 jit_solution(2413280010600079240)
XLA Ops:
  0.0 69.5 %shard_map.109 = bf16[512,512]{1,0:T(8,128)(2,1)} custom-call(bf16[512,512]{1,0:T(8,128)(2,1)} %tok_hbm.1, bf16[16,256]{1,0:T(8,128)(2,1)} %wq_hbm.1, bf16[16,64]{1,0:T(8,128)(2,1)} %wk_hbm.1, bf16[16,64]{1,0:T(8,128)(2,1)} %wv_hbm.1, bf16[16,256]{1,0:T(8,128)(2,1)} %wc_hbm.1, f32[1,4]{1,0:T(1,128)} %bitcast.9, bf16[1,256,256]{2,1,0:T(8,128)(2,1)} %wpool_hbm.1, ...), custom_call_target="tpu_custom_call" | custom-call | tf_op jit(solution)/shard_map/pallas_call | solution.py:465
  69.6 1.9 %copy.13 = bf16[512,512]{1,0:T(8,128)(2,1)} copy(bf16[512,512]{1,0:T(8,128)(2,1)} %shard_map.109) | data formatting | bytes 1048576

commit v6 on v5

--- a/solution.py
+++ b/solution.py
@@ -16,8 +16,8 @@
 epsilon = 1e-05
 masked_score = -1e30
 
-OWN, NEAR, FAR = 4, (0, 9), (9, 16)
-FIRST, SECOND, THIRD = ((2, 5), (5, 7)), ((0, 2), (7, 9)), ((9, 12), (12, 16))
+OWN, NEAR, REST = 3, (0, 7), (7, 16)
+FIRST, SECOND, MIDDLE, FAR = ((1, 4), (4, 6)), ((0, 1), (6, 7)), ((7, 10), (13, 16)), ((10, 12), (12, 13))
 NT = (((1,), (1,)), ((), ()))
 TN = (((0,), (0,)), ((), ()))
 BF16, F32 = jnp.bfloat16, jnp.float32
@@ -55,7 +55,7 @@
             "sp_2": lax.rem(s, NC),
         }
 
-    peers = [dev_z(d) for d in (4, -4, 3, -3, 2, -2, 1, -1)]
+    peers = [dev_z(d) for d in (3, -3, 2, -2, 1, -1)]
     peers += [dev_y(2), dev_sp(1), dev_sp(-1), dev_x(1), dev_x(-1), dev_y(1), dev_y(-1), dev_c]
     mine_in, mine_out = win.at[OWN], wout.at[OWN]
     pairs = (
@@ -112,36 +112,44 @@
         def wait(self, slots, got):
             waiting(self.w.at[pl.ds(0, slots)], "recv", self.name + got)
 
+        def pass_on(self, src, dst, d, got):
+            self.send(self.at(0, 0, src, src + 1), self.at(0, 0, dst, dst + 1), dev_z(d), got)
+
         def near(self):
-            for d in (1, -1, 2, -2, 4, -4, 3, -3):
-                p = (4 - d) % NZ
-                got = {4: "m4", -4: "p4", 3: "n3", -3: "n3"}.get(d, "n1")
-                self.send(self.at(0, 0, OWN, OWN + 1), self.at(0, 0, p, p + 1), dev_z(d), got)
+            for d in (1, -1, 2, -2, 3, -3):
+                self.pass_on(OWN, (3 - d) % NZ, d, {3: "m3", -3: "p3"}.get(d, "n1"))
+
+        def middle(self):
+            self.wait(1, "m3")
+            for e in (3, 2, 1):
+                self.pass_on(0, 16 - e, e, "m6" if e == 3 else "mid")
+            self.wait(1, "p3")
+            for e in (3, 2, 1):
+                self.pass_on(6, 6 + e, -e, "p6" if e == 3 else "mid")
 
         def far(self):
-            self.wait(1, "m4")
-            for e in (4, 3, 2, 1):
-                self.send(self.at(0, 0, 0, 1), self.at(0, 0, 16 - e, 17 - e), dev_z(e), "far")
-            self.wait(1, "p4")
-            for e in (3, 2, 1):
-                self.send(self.at(0, 0, 8, 9), self.at(0, 0, 8 + e, 9 + e), dev_z(-e), "far")
+            self.wait(1, "m6")
+            self.pass_on(13, 11, 2, "far")
+            self.pass_on(13, 12, 1, "far")
+            self.wait(1, "p6")
+            self.pass_on(9, 10, -1, "far")
 
         def along_x(self, stage):
             up, down = stage
-            others = "o%d" % (stage is THIRD)
+            others = "o%d" % (stage in (MIDDLE, FAR))
             self.send(self.at(0, 0, *up), self.at(3, 0, *up), dev_x(1), "x%d" % up[0])
             self.send(self.at(0, 0, *down), self.at(1, 0, *down), dev_x(-1), "x%d" % down[0])
             self.send(self.at(0, 0, *down), self.at(3, 0, *down), dev_x(1), others)
             self.send(self.at(0, 0, *up), self.at(1, 0, *up), dev_x(-1), others)
 
         def relay_x(self, stage):
-            part = "rest" if stage is THIRD else "near"
+            part = "rest" if stage in (MIDDLE, FAR) else "near"
             for r, d, span in ((3, 1, stage[0]), (1, -1, stage[1])):
                 self.wait(span[1] - span[0], "x%d" % span[0])
                 self.send(self.at(r, 0, *span), self.at(2, 0, *span), dev_x(d), "x2" + part)
 
         def across(self, r, span):
-            part = "near" if span[0] < 9 else "rest"
+            part = "near" if span == NEAR else "rest"
             self.send(self.at(r, 0, *span), self.at(r, 1, *span), dev_c, "c" + part)
 
         def first(self):
@@ -149,39 +157,42 @@
             self.along_x(FIRST)
 
         def second(self):
-            self.wait(2, "n3")
             self.along_x(SECOND)
             self.across(0, NEAR)
 
         def third(self):
-            self.wait(7, "far")
-            self.along_x(THIRD)
-            self.across(0, FAR)
+            self.wait(4, "mid")
+            self.along_x(MIDDLE)
+
+        def fourth(self):
+            self.wait(3, "far")
+            self.along_x(FAR)
+            self.across(0, REST)
 
         def others_near(self):
-            self.wait(9, "o0")
+            self.wait(7, "o0")
             self.across(3, NEAR)
             self.across(1, NEAR)
 
-        def others_far(self):
-            self.wait(7, "o1")
-            self.across(3, FAR)
-            self.across(1, FAR)
+        def others_rest(self):
+            self.wait(9, "o1")
+            self.across(3, REST)
+            self.across(1, REST)
 
         def last_near(self):
-            self.wait(9, "x2near")
+            self.wait(7, "x2near")
             self.across(2, NEAR)
 
-        def last_far(self):
-            self.wait(7, "x2rest")
-            self.across(2, FAR)
+        def last_rest(self):
+            self.wait(9, "x2rest")
+            self.across(2, REST)
 
         def in_order(self, dest, span, turned):
             w = self.w
-            self.wait(NX * (span[1] - span[0]), "cnear" if span[0] < 9 else "crest")
+            self.wait(NX * (span[1] - span[0]), "cnear" if span == NEAR else "crest")
 
             def one(p, carry):
-                base = (lax.rem(z + p + (NZ - 4), NZ) if turned else p) * (NX * NC * 16)
+                base = (lax.rem(z + p + (NZ - OWN), NZ) if turned else p) * (NX * NC * 16)
                 for r in range(NX):
                     for k in range(NC):
                         at = base + lax.rem(x + r, NX) * (NC * 16) + lax.rem(c + k, NC) * 16
@@ -220,8 +231,8 @@
             tokens_to(1, b, 0, -1, "tok")
     with jax.named_scope("in_first"):
         into.first()
-    with jax.named_scope("in_far"):
-        into.far()
+    with jax.named_scope("in_middle"):
+        into.middle()
         outof.near()
         for load in loads[7:]:
             load.wait()
@@ -232,59 +243,73 @@
         tokens_relay(2)
     with jax.named_scope("in_relay_first"):
         into.relay_x(FIRST)
+    with jax.named_scope("in_far"):
+        into.far()
+    with jax.named_scope("in_third"):
+        into.third()
     with jax.named_scope("tok_relay_b"):
         tokens_relay(1)
         tokens_relay(3)
     with jax.named_scope("in_relay_second"):
         into.relay_x(SECOND)
-    with jax.named_scope("in_third"):
-        into.third()
+    with jax.named_scope("out_middle"):
+        outof.middle()
     with jax.named_scope("in_others_near"):
         into.others_near()
-    with jax.named_scope("out_far"):
-        outof.far()
+    with jax.named_scope("in_fourth"):
+        into.fourth()
+    with jax.named_scope("in_relay_third"):
+        into.relay_x(MIDDLE)
     with jax.named_scope("out_first"):
         outof.first()
     with jax.named_scope("in_last_near"):
         into.last_near()
-    with jax.named_scope("in_relay_third"):
-        into.relay_x(THIRD)
+    with jax.named_scope("out_far"):
+        outof.far()
+    with jax.named_scope("in_relay_fourth"):
+        into.relay_x(FAR)
     with jax.named_scope("out_second"):
         outof.second()
+    with jax.named_scope("in_others_rest"):
+        into.others_rest()
+    with jax.named_scope("out_third"):
+        outof.third()
     with jax.named_scope("in_order_near"):
         into.in_order(win_abs, NEAR, False)
-    with jax.named_scope("in_others_far"):
-        into.others_far()
-    with jax.named_scope("out_relay_first"):
-        outof.relay_x(FIRST)
-    with jax.named_scope("out_third"):
-        outof.third()
-    with jax.named_scope("in_last_far"):
-        into.last_far()
+    with jax.named_scope("out_fourth"):
+        outof.fourth()
     with jax.named_scope("tok_done"):
         waiting(toks.at[pl.ds(0, 2)], "recv", "tok")
         for p in range(NZ):
-            at = lax.rem(z + (p + NZ - 4), NZ)
+            at = lax.rem(z + (p + NZ - OWN), NZ)
             per = feats // 128
             r = lax.rem(lax.div(at, per) + (NY - y), NY)
             cols = pl.ds(pl.multiple_of(lax.rem(at, per) * 128, 128), 128)
             turned_toks[:, p * 128 : (p + 1) * 128] = toks[r, :, cols]
 
+    with jax.named_scope("out_relay_first"):
+        outof.relay_x(FIRST)
+    with jax.named_scope("in_last_rest"):
+        into.last_rest()
+    with jax.named_scope("out_relay_second"):
+        outof.relay_x(SECOND)
+    with jax.named_scope("out_relay_third"):
+        outof.relay_x(MIDDLE)
+        outof.others_near()
     parts = ((256, 384), (384, 640), (0, 256))
     with jax.named_scope("project_near"):
         depth = slice(NEAR[0] * 128, NEAR[1] * 128)
         for lo, hi in parts:
             acc[:, lo:hi] = jnp.dot(turned_toks[:, depth], win_abs[depth, lo:hi], preferred_element_type=F32)
-    with jax.named_scope("out_relay_second"):
-        outof.relay_x(SECOND)
-        outof.others_near()
-    with jax.named_scope("in_order_far"):
-        into.in_order(win_abs, FAR, False)
-    with jax.named_scope("out_relay_third"):
-        outof.relay_x(THIRD)
+    with jax.named_scope("in_order_rest"):
+        into.in_order(win_abs, REST, False)
+
+    with jax.named_scope("out_relay_fourth"):
+        outof.relay_x(FAR)
+        outof.others_rest()
 
     def project(lo, hi):
-        depth = slice(FAR[0] * 128, FAR[1] * 128)
+        depth = slice(REST[0] * 128, REST[1] * 128)
         return acc[:, lo:hi] + jnp.dot(turned_toks[:, depth], win_abs[depth, lo:hi], preferred_element_type=F32)
 
     own_kv, own_ch = (kv, WINDOW, "kv"), (chan, RIM, "ch")
@@ -299,9 +324,9 @@
         query[...] = (project(0, 256) * HEAD_DIM ** (-0.5)).astype(BF16)
         to_neighbours(*own_kv)
         to_neighbours(*own_ch)
+
     with jax.named_scope("out_last_near"):
         outof.last_near()
-        outof.others_far()
 
     half = lax.shift_left(jnp.int32(1), y.astype(jnp.int32))
     sinks = jnp.concatenate([jnp.broadcast_to(sink[0:1, h : h + 1], (1, WINDOW)) for h in range(4)], axis=1)
@@ -376,14 +401,14 @@
 
     with jax.named_scope("mix1"):
         mixers(1)
-    with jax.named_scope("out_last_far"):
-        outof.last_far()
+    with jax.named_scope("out_last_rest"):
+        outof.last_rest()
     with jax.named_scope("mix2"):
         mixers(2)
     with jax.named_scope("out_order_near"):
         outof.in_order(wout_abs, NEAR, True)
-    with jax.named_scope("out_order_far"):
-        outof.in_order(wout_abs, FAR, True)
+    with jax.named_scope("out_order_rest"):
+        outof.in_order(wout_abs, REST, True)
     with jax.named_scope("part12"):
         partials(0, 1, 2)
     with jax.named_scope("halo"):
@@ -453,7 +478,7 @@
     assert len(groups) == SEMAPHORES
 
 
-SEMAPHORES = 57
+SEMAPHORES = 65
 
 
 def local(tokens, w_query, w_key, w_value, w_pool_in, sink, w_pool, pool_scale, w_out_attn, w_out_pool, out_gain):

time: 71.7 us -> 70.7 us (0.986)
  Pallas kernels: 69.5 us -> 68.6 us
    pallas_call x1, Pallas kernels: 69.5 us -> 68.6 us  [local(): pl.pallas_call(kernel, out_shape=jax.ShapeDtypeStruct((rows, feats), BF16...]
where the time goes in v6:
time: 70.7 us; the launch traced here: 70.5 us
  Pallas kernels  68.6 us (97%)
  local copies, waits for them, and re-layouts  1.87 us (3%)
    pallas_call x1, Pallas kernels, local(): pl.pallas_call(kernel, out_shape=jax.ShapeDtypeStruct((rows, feats), BF16...  68.6 us
    unnamed x1, local copies, waits for them, and re-layouts  1.87 us

profile of v6, /device:TPU:1, one launch (start us, length us, event | category | flops | bytes accessed | tf_op | source)
XLA Modules:
  0.0 70.5 jit_solution(9986557631595750052)
XLA Ops:
  0.0 68.6 %shard_map.109 = bf16[512,512]{1,0:T(8,128)(2,1)} custom-call(bf16[512,512]{1,0:T(8,128)(2,1)} %tok_hbm.1, bf16[16,256]{1,0:T(8,128)(2,1)} %wq_hbm.1, bf16[16,64]{1,0:T(8,128)(2,1)} %wk_hbm.1, bf16[16,64]{1,0:T(8,128)(2,1)} %wv_hbm.1, bf16[16,256]{1,0:T(8,128)(2,1)} %wc_hbm.1, f32[1,4]{1,0:T(1,128)} %bitcast.9, bf16[1,256,256]{2,1,0:T(8,128)(2,1)} %wpool_hbm.1, ...), custom_call_target="tpu_custom_call" | custom-call | tf_op jit(solution)/shard_map/pallas_call | solution.py:490
  68.6 1.9 %copy.13 = bf16[512,512]{1,0:T(8,128)(2,1)} copy(bf16[512,512]{1,0:T(8,128)(2,1)} %shard_map.109) | data formatting | bytes 1048576

commit v7 on v6

--- a/solution.py
+++ b/solution.py
@@ -293,14 +293,14 @@
         into.last_rest()
     with jax.named_scope("out_relay_second"):
         outof.relay_x(SECOND)
-    with jax.named_scope("out_relay_third"):
-        outof.relay_x(MIDDLE)
-        outof.others_near()
     parts = ((256, 384), (384, 640), (0, 256))
     with jax.named_scope("project_near"):
         depth = slice(NEAR[0] * 128, NEAR[1] * 128)
         for lo, hi in parts:
             acc[:, lo:hi] = jnp.dot(turned_toks[:, depth], win_abs[depth, lo:hi], preferred_element_type=F32)
+    with jax.named_scope("out_relay_third"):
+        outof.relay_x(MIDDLE)
+        outof.others_near()
     with jax.named_scope("in_order_rest"):
         into.in_order(win_abs, REST, False)
 
@@ -374,19 +374,24 @@
 
     def partials(p, first, second):
         both = jnp.concatenate([hid[chunk(first), :], hid[chunk(second), :]], axis=0)
-        for d in (2, 3, 1, 0):
+
+        def terms(d):
             cols = pl.ds(pl.multiple_of(lax.rem(y + d, NY) * feats, feats), feats)
-            terms = lax.dot_general(both, wout_abs[cols, :], NT, preferred_element_type=F32).astype(BF16)
-            part[d, chunk(first), :] = terms[:WINDOW]
-            part[d, chunk(second), :] = terms[WINDOW:]
+            out = lax.dot_general(both, wout_abs[cols, :], NT, preferred_element_type=F32).astype(BF16)
+            part[d, chunk(first), :] = out[:WINDOW]
+            part[d, chunk(second), :] = out[WINDOW:]
+
+        terms(2)
         for n in (first, second):
             target = dev_y(1 if n < 2 else -1)
             message(part.at[2, chunk(n)], relayed.at[chunk(n)], target, "sum", "via%d" % n).start()
+        for d in (3, 1, 0):
+            terms(d)
         for n in (first, second):
             if n < 2:
-                message(part.at[3, chunk(n)], from_next.at[chunk(n)], dev_y(-1), "sum", "sum%d" % p).start()
+                message(part.at[3, chunk(n)], from_next.at[chunk(n)], dev_y(-1), "sum", "one%d" % p).start()
             else:
-                message(part.at[1, chunk(n)], from_prev.at[chunk(n)], dev_y(1), "sum", "sum%d" % p).start()
+                message(part.at[1, chunk(n)], from_prev.at[chunk(n)], dev_y(1), "sum", "one%d" % p).start()
 
     def relay(n):
         at = chunk(n)
@@ -418,20 +423,20 @@
         mixers(0, 3)
     with jax.named_scope("part03"):
         partials(1, 0, 3)
-    with jax.named_scope("relay12"):
-        relay(1)
-        relay(2)
-    with jax.named_scope("relay03"):
-        relay(0)
-        relay(3)
-
     lane = lax.broadcasted_iota(jnp.int32, (WINDOW, 128), 1)
 
+    def prepare(p, first, second):
+        waiting(from_prev.at[pl.ds(0, 2 * WINDOW)], "recv", "one%d" % p)
+        for n in (first, second):
+            at = chunk(n)
+            single = (from_next if n < 2 else from_prev)[at, :]
+            share[at, :] = part[0, at, :].astype(F32) + single.astype(F32)
+
     def settle(p, first, second):
-        waiting(from_prev, "recv", "sum%d" % p)
+        waiting(from_prev.at[pl.ds(0, 2 * WINDOW)], "recv", "sum%d" % p)
         for k, n in enumerate((first, second)):
             at = chunk(n)
-            mix = part[0, at, :].astype(F32) + from_prev[at, :].astype(F32) + from_next[at, :].astype(F32)
+            mix = share[at, :] + (from_prev if n < 2 else from_next)[at, :].astype(F32)
             share[at, :] = mix
             one = jnp.sum(mix, axis=1, keepdims=True)
             two = jnp.sum(mix * mix, axis=1, keepdims=True)
@@ -458,6 +463,14 @@
             writes.append(pltpu.make_async_copy(outv.at[at], out_hbm.at[at], out_sem.at[n]))
             writes[-1].start()
 
+    with jax.named_scope("relay12"):
+        relay(1)
+        relay(2)
+        prepare(0, 1, 2)
+    with jax.named_scope("relay03"):
+        relay(0)
+        relay(3)
+        prepare(1, 0, 3)
     with jax.named_scope("settle12"):
         settle(0, 1, 2)
     with jax.named_scope("settle03"):
@@ -478,7 +491,7 @@
     assert len(groups) == SEMAPHORES
 
 
-SEMAPHORES = 65
+SEMAPHORES = 67
 
 
 def local(tokens, w_query, w_key, w_value, w_pool_in, sink, w_pool, pool_scale, w_out_attn, w_out_pool, out_gain):

time: 70.7 us -> 70.2 us (level)
  no operation moved by 1% of the time
where the time goes in v7:
time: 70.2 us; the launch traced here: 70.1 us
  Pallas kernels  68.2 us (97%)
  local copies, waits for them, and re-layouts  1.87 us (3%)
    pallas_call x1, Pallas kernels, local(): pl.pallas_call(kernel, out_shape=jax.ShapeDtypeStruct((rows, feats), BF16...  68.2 us
    unnamed x1, local copies, waits for them, and re-layouts  1.87 us

profile of v7, /device:TPU:1, one launch (start us, length us, event | category | flops | bytes accessed | tf_op | source)
XLA Modules:
  0.0 70.1 jit_solution(12851415561317671891)
XLA Ops:
  0.0 68.2 %shard_map.109 = bf16[512,512]{1,0:T(8,128)(2,1)} custom-call(bf16[512,512]{1,0:T(8,128)(2,1)} %tok_hbm.1, bf16[16,256]{1,0:T(8,128)(2,1)} %wq_hbm.1, bf16[16,64]{1,0:T(8,128)(2,1)} %wk_hbm.1, bf16[16,64]{1,0:T(8,128)(2,1)} %wv_hbm.1, bf16[16,256]{1,0:T(8,128)(2,1)} %wc_hbm.1, f32[1,4]{1,0:T(1,128)} %bitcast.9, bf16[1,256,256]{2,1,0:T(8,128)(2,1)} %wpool_hbm.1, ...), custom_call_target="tpu_custom_call" | custom-call | tf_op jit(solution)/shard_map/pallas_call | solution.py:503
  68.2 1.9 %copy.13 = bf16[512,512]{1,0:T(8,128)(2,1)} copy(bf16[512,512]{1,0:T(8,128)(2,1)} %shard_map.109) | data formatting | bytes 1048576

commit v8 on v7

--- a/solution.py
+++ b/solution.py
@@ -451,17 +451,20 @@
     def finish(p, first, second):
         waiting(stats.at[pl.ds(0, 3)], "recv", "told%d" % p)
         for k, n in enumerate((first, second)):
-            at = chunk(n)
             eight = slice(k * 8, k * 8 + 8)
             both = stats[4 * p, eight, :] + stats[4 * p + 1, eight, :]
             both = both + stats[4 * p + 2, eight, :] + stats[4 * p + 3, eight, :]
             both = jnp.concatenate([both] * 16, axis=0).T
             mean = both[:, 0:1] / width
             variance = both[:, 1:2] / width - mean * mean
-            normed = (share[at, :] - mean) * lax.rsqrt(variance + epsilon) * gain[...]
-            outv[at, :] = normed.astype(BF16)
-            writes.append(pltpu.make_async_copy(outv.at[at], out_hbm.at[at], out_sem.at[n]))
-            writes[-1].start()
+            rise = lax.rsqrt(variance + epsilon)
+            for m in range(2):
+                top, size = m * (WINDOW // 2), WINDOW // 2
+                at = pl.ds(n * WINDOW + top, size)
+                normed = (share[at, :] - mean[top : top + size]) * rise[top : top + size] * gain[...]
+                outv[at, :] = normed.astype(BF16)
+                writes.append(pltpu.make_async_copy(outv.at[at], out_hbm.at[at], out_sem.at[2 * n + m]))
+                writes[-1].start()
 
     with jax.named_scope("relay12"):
         relay(1)
@@ -532,7 +535,7 @@
             pltpu.VMEM((1, 512), F32),
             pltpu.VMEM((rows, feats), BF16),
             pltpu.SemaphoreType.DMA((11,)),
-            pltpu.SemaphoreType.DMA((4,)),
+            pltpu.SemaphoreType.DMA((8,)),
             pltpu.SemaphoreType.DMA((SEMAPHORES,)),
         ],
         compiler_params=pltpu.CompilerParams(

time: 70.2 us -> 70.2 us (level)
  no operation moved by 1% of the time
where the time goes in v8:
time: 70.2 us; the launch traced here: 70.1 us
  Pallas kernels  68.2 us (97%)
  local copies, waits for them, and re-layouts  1.87 us (3%)
    pallas_call x1, Pallas kernels, local(): pl.pallas_call(kernel, out_shape=jax.ShapeDtypeStruct((rows, feats), BF16...  68.2 us
    unnamed x1, local copies, waits for them, and re-layouts  1.87 us

profile of v8, /device:TPU:1, one launch (start us, length us, event | category | flops | bytes accessed | tf_op | source)
XLA Modules:
  0.0 70.1 jit_solution(2247514968395656442)
XLA Ops:
  0.0 68.2 %shard_map.109 = bf16[512,512]{1,0:T(8,128)(2,1)} custom-call(bf16[512,512]{1,0:T(8,128)(2,1)} %tok_hbm.1, bf16[16,256]{1,0:T(8,128)(2,1)} %wq_hbm.1, bf16[16,64]{1,0:T(8,128)(2,1)} %wk_hbm.1, bf16[16,64]{1,0:T(8,128)(2,1)} %wv_hbm.1, bf16[16,256]{1,0:T(8,128)(2,1)} %wc_hbm.1, f32[1,4]{1,0:T(1,128)} %bitcast.9, bf16[1,256,256]{2,1,0:T(8,128)(2,1)} %wpool_hbm.1, ...), custom_call_target="tpu_custom_call" | custom-call | tf_op jit(solution)/shard_map/pallas_call | solution.py:506
  68.2 1.9 %copy.13 = bf16[512,512]{1,0:T(8,128)(2,1)} copy(bf16[512,512]{1,0:T(8,128)(2,1)} %shard_map.109) | data formatting | bytes 1048576
